TPU v7x, 32 devices: a whole 2x2x4 slice. The times are simulated.
32 devices in a mesh: sp: 16 (over z, y, x), tp: 2 (over core).
Axes of the slice: x: 2, y: 2, z: 4, core: 2. Of those that a mesh axis runs over, the one named last changes fastest.
Arguments:
- queries_narrow: bfloat16 [4096, 1024], P('sp', 'tp'), may hold values from -40 to 40
- keys_narrow: bfloat16 [4096, 256], P('sp', 'tp'), may hold values from -40 to 40
- values_narrow: bfloat16 [4096, 256], P('sp', 'tp'), may hold values from -6 to 6
- queries_wide: bfloat16 [4096, 1024], P('sp', 'tp'), may hold values from -40 to 40
- keys_wide: bfloat16 [4096, 512], P('sp', 'tp'), may hold values from -40 to 40
- values_wide: bfloat16 [4096, 512], P('sp', 'tp'), may hold values from -6 to 6
- lambda_narrow: float32 [8], P('tp'), may hold values from 0.3 to 0.8
- lambda_wide: float32 [4], P('tp'), may hold values from 0.3 to 0.8
- gain_narrow: float32 [128], replicated, may hold values from 0.1 to 1.9
- gain_wide: float32 [256], replicated, may hold values from 0.1 to 1.9
- out_narrow: bfloat16 [1024, 2048], replicated, may hold values from -0.125 to 0.125
- out_wide: bfloat16 [1024, 2048], replicated, may hold values from -0.125 to 0.125
- stream: bfloat16 [4096, 2048], P(('sp', 'tp')), may hold values from -6 to 6
- gain_mix: float32 [2048], replicated, may hold values from 0.1 to 1.9
- gain_ffn: float32 [2048], replicated, may hold values from 0.1 to 1.9
- gain_post: float32 [2048], replicated, may hold values from 0.1 to 1.9
- shared_gate: bfloat16 [2048, 512], replicated, may hold values from -0.125 to 0.125
- shared_up: bfloat16 [2048, 512], replicated, may hold values from -0.125 to 0.125
- shared_down: bfloat16 [512, 2048], replicated, may hold values from -0.25 to 0.25
- expert_gate: bfloat16 [32, 2048, 512], P('sp', None, 'tp'), may hold values from -0.125 to 0.125
- expert_up: bfloat16 [32, 2048, 512], P('sp', None, 'tp'), may hold values from -0.125 to 0.125
- expert_down: bfloat16 [32, 512, 2048], P('sp', 'tp'), may hold values from -0.25 to 0.25
- expert_ids: int32 [4096, 4], P(('sp', 'tp')), may hold values from 0 to 31, all different within a row; in each aligned block of 128 rows (0 to 127, 128 to 255, ...) at most 24 rows name the same one
- route_weights: float32 [4096, 4], P(('sp', 'tp')), may hold values from 0.2 to 1
Outputs:
- layer_out: bfloat16 [4096, 2048], P(('sp', 'tp'))
Inputs may be any that keep to these rules, and one draw needn't show every extreme that they name: `expert_ids`: the experts of one token differ. Within the rows that one device holds (aligned blocks of rows in the placement's order), no expert is named more than 24 times, and in every draw some expert is named exactly 24 times there.
All inputs are finite; a program needn't handle non-finite values.
Results may differ from a plain program's by a relative error of at most 0.015.
Values may be sent and summed in bfloat16 or wider, within the bound.
A program may use at most 192 MiB of HBM per device.

v0:
```python
import functools
import math

import jax
import jax.numpy as jnp
from jax import lax
from jax.experimental import pallas as pl
from jax.experimental.pallas import tpu as pltpu
from jax.sharding import PartitionSpec as P

D = 2048
DN = 64
VN = 128
DW = 128
VW = 256
TOPK = 4


EPS = 1e-06


def rms_scale(values, gain_row):
    return values * lax.rsqrt(jnp.mean(values * values, axis=-1, keepdims=True) + EPS) * gain_row


MESH = pl.DeviceIdType.MESH
LOG2E = math.log2(math.e)
MASKED = -1e30


def plane_shape(sp_count):
    bits = sp_count.bit_length() - 1
    if 1 << bits != sp_count:
        return sp_count, 1, 1
    columns = 1 << (bits // 3 if bits % 3 == 0 else (bits - bits // 2) // 2)
    rows = columns
    return sp_count // (rows * columns), rows, columns


def attend_kernel(
    dims,
    qn_ref,
    kn_ref,
    vn_ref,
    qw_ref,
    kw_ref,
    vw_ref,
    lamn_ref,
    lamw_ref,
    gainn_ref,
    gainw_ref,
    out_ref,
    kv,
    att,
    row_max,
    row_sum,
    acc_n,
    acc_w,
    load_sem,
    recv_sem,
    up_sem,
    first_sem,
    second_sem,
    pair_send,
    pair_recv,
    pair_ready,
):
    planes, rows, columns, tp_count = dims
    per_plane = rows * columns
    sp = lax.axis_index("sp")
    tp = lax.axis_index("tp")
    plane = sp // per_plane
    cell = sp % per_plane
    y = cell // columns
    x = cell % columns
    queries = qn_ref.shape[2]
    half_rows = queries // 2

    own = []
    begin = 0
    for index, ref in enumerate((kn_ref, vn_ref, kw_ref, vw_ref)):
        width = ref.shape[1]
        own.append(
            pltpu.make_async_copy(ref, kv.at[0, cell, :, pl.ds(begin, width)], load_sem.at[index])
        )
        begin += width
    for copy in own:
        copy.start()

    def line(axis):
        if axis == 0:
            return [((y + k) % rows) * columns + x for k in range(1, rows)]
        return [y * columns + (x + k) % columns for k in range(1, columns)]

    def crossed(other, axis):
        oy = other // columns
        ox = other % columns
        if axis == 0:
            return [((oy + k) % rows) * columns + ox for k in range(1, rows)]
        return [oy * columns + (ox + k) % columns for k in range(1, columns)]

    barrier = pltpu.get_barrier_semaphore()
    for other in line(0) + line(1):
        pl.semaphore_signal(
            barrier, inc=1, device_id={"sp": plane * per_plane + other}, device_id_type=MESH
        )
    for k in range(1, tp_count):
        pl.semaphore_signal(
            barrier, inc=1, device_id={"tp": (tp + k) % tp_count}, device_id_type=MESH
        )

    @pl.when(plane > 0)
    def _():
        pl.semaphore_signal(barrier, inc=1, device_id={"sp": sp - per_plane}, device_id_type=MESH)

    @pl.when(plane < planes - 1)
    def _():
        pl.semaphore_signal(barrier, inc=1, device_id={"sp": sp + per_plane}, device_id_type=MESH)

    below = (plane > 0).astype(jnp.int32)
    above = (plane < planes - 1).astype(jnp.int32)
    pl.semaphore_wait(barrier, rows - 1 + columns - 1 + tp_count - 1 + below + above)

    for copy in own:
        copy.wait()

    def piece(depth, block, half):
        return kv.at[depth, block, pl.ds(half * half_rows, half_rows), :]

    def remote(depth, to_depth, block, half, target, send):
        return pltpu.make_async_remote_copy(
            src_ref=piece(depth, block, half),
            dst_ref=piece(to_depth, block, half),
            send_sem=send,
            recv_sem=recv_sem.at[to_depth, block, half],
            device_id={"sp": target},
            device_id_type=MESH,
        )

    def arrived(depth, block, half):
        pltpu.make_async_remote_copy(
            src_ref=piece(depth, block, half),
            dst_ref=piece(depth, block, half),
            send_sem=up_sem.at[0, 0],
            recv_sem=recv_sem.at[depth, block, half],
            device_id={"sp": sp},
            device_id_type=MESH,
        ).wait_recv()

    def up_copies(depth):
        return [
            remote(depth, depth + 1, cell, half, sp + per_plane, up_sem.at[depth, half])
            for half in range(2)
        ]

    def direct_copies(depth):
        copies = []
        for half in range(2):
            for k, other in enumerate(line(half)):
                copies.append(
                    remote(
                        depth,
                        depth,
                        cell,
                        half,
                        plane * per_plane + other,
                        first_sem.at[depth, half, k],
                    )
                )
            for k, other in enumerate(line(1 - half)):
                copies.append(
                    remote(
                        depth,
                        depth,
                        cell,
                        half,
                        plane * per_plane + other,
                        second_sem.at[depth, half, 0, k],
                    )
                )
        return copies

    def relay_copies(depth):
        groups = []
        for half in range(2):
            for i, block in enumerate(line(half)):
                copies = [
                    remote(
                        depth,
                        depth,
                        block,
                        half,
                        plane * per_plane + other,
                        second_sem.at[depth, half, i + 1, k],
                    )
                    for k, other in enumerate(line(1 - half))
                ]
                groups.append((block, half, copies))
        return groups

    def issue(depth):
        @pl.when(plane < planes - 1)
        def _():
            for copy in up_copies(depth):
                copy.start()

        for copy in direct_copies(depth):
            copy.start()

    def relay(depth):
        for block, half, copies in relay_copies(depth):
            arrived(depth, block, half)
            for copy in copies:
                copy.start()

    def finish(depth):
        for half in range(2):
            for block in line(1 - half):
                arrived(depth, block, half)
            for first in line(half):
                for block in crossed(first, 1 - half):
                    arrived(depth, block, half)

    row_max[...] = jnp.full_like(row_max, MASKED)
    row_sum[...] = jnp.zeros_like(row_sum)
    acc_n[...] = jnp.zeros_like(acc_n)
    acc_w[...] = jnp.zeros_like(acc_w)
    heads_n = qn_ref.shape[0]
    heads_w = qw_ref.shape[1] // kw_ref.shape[1]
    width_k = kn_ref.shape[1]
    value_n = vn_ref.shape[1]
    begin_kw = width_k + value_n
    map_w = kw_ref.shape[1] // 2
    begin_vw = begin_kw + 2 * map_w
    value_w = vw_ref.shape[1]
    chunk = math.gcd(per_plane, 4)
    key_rows = chunk * queries

    def tile(query, key, value, factor, mask, state, acc, slot):
        scores = lax.dot_general(
            query, key, (((1,), (1,)), ((), ())), preferred_element_type=jnp.float32
        )
        if mask is not None:
            scores = jnp.where(mask, scores, MASKED)
        before = row_max[state][:, :1]
        now = jnp.maximum(before, jnp.max(scores, axis=1, keepdims=True))
        weights = jnp.exp2((scores - now) * factor)
        decay = jnp.exp2((before - now) * factor)
        total = row_sum[state][:, :1] * decay + jnp.sum(weights, axis=1, keepdims=True)
        acc[slot] = acc[slot] * decay + jnp.dot(
            weights.astype(jnp.bfloat16), value, preferred_element_type=jnp.float32
        )
        row_max[state] = jnp.broadcast_to(now, row_max.shape[1:])
        row_sum[state] = jnp.broadcast_to(total, row_sum.shape[1:])

    def attend(depth, masked):
        def part(at):
            def columns_of(begin, width):
                return kv[depth, pl.ds(at, chunk), :, begin : begin + width].reshape(
                    key_rows, width
                )

            mask = None
            if masked:
                query_pos = cell * queries + lax.broadcasted_iota(
                    jnp.int32, (queries, key_rows), 0
                )
                key_pos = at * queries + lax.broadcasted_iota(jnp.int32, (queries, key_rows), 1)
                mask = key_pos <= query_pos

            def narrow(head, carry):
                key = columns_of(0, width_k)
                value = columns_of(width_k, value_n)
                for which in range(2):
                    index = head * 2 + which
                    tile(
                        qn_ref[head, which],
                        key,
                        value,
                        DN**-0.5 * LOG2E,
                        mask,
                        index,
                        acc_n,
                        index,
                    )
                return carry

            def wide(head, carry):
                value = columns_of(begin_vw, value_w)
                for which in range(2):
                    index = head * 2 + which
                    tile(
                        qw_ref[:, pl.ds(pl.multiple_of(index * map_w, map_w), map_w)],
                        columns_of(begin_kw + which * map_w, map_w),
                        value,
                        DW**-0.5 * LOG2E,
                        mask,
                        2 * heads_n + index,
                        acc_w,
                        index,
                    )
                return carry

            lax.fori_loop(0, heads_n, narrow, 0)
            lax.fori_loop(0, heads_w, wide, 0)

        if per_plane == chunk:
            part(0)
        else:

            def step(at, carry):
                part(at * chunk)
                return carry

            lax.fori_loop(0, per_plane // chunk, step, 0)

    def advance(depth):
        @pl.when(depth < plane)
        def _():
            for half in range(2):
                arrived(depth + 1, cell, half)
            issue(depth + 1)

    def relay_next(depth):
        @pl.when(depth < plane)
        def _():
            relay(depth + 1)

    issue(0)
    relay(0)
    advance(0)
    finish(0)
    attend(0, True)
    relay_next(0)

    def depth_step(depth, carry):
        advance(depth)
        finish(depth)
        attend(depth, False)
        relay_next(depth)
        return carry

    lax.fori_loop(1, plane + 1, depth_step, 0)

    def close(first, second, lam, gain):
        head = first - lam * second
        scale = lax.rsqrt(jnp.mean(head * head, axis=1, keepdims=True) + EPS)
        return (head * scale * gain).astype(jnp.bfloat16)

    for head in range(heads_n):
        maps = [acc_n[2 * head + k] / row_sum[2 * head + k][:, :1] for k in range(2)]
        att[:, head * value_n : (head + 1) * value_n] = close(
            maps[0], maps[1], lamn_ref[head], gainn_ref[...]
        )
    begin_w = heads_n * value_n
    for head in range(heads_w):
        maps = [
            acc_w[2 * head + k] / row_sum[2 * (heads_n + head) + k][:, :1] for k in range(2)
        ]
        att[:, begin_w + head * value_w : begin_w + (head + 1) * value_w] = close(
            maps[0], maps[1], lamw_ref[head], gainw_ref[...]
        )

    def drain(depth, carry):
        @pl.when(plane < planes - 1)
        def _():
            for copy in up_copies(depth):
                copy.wait_send()

        for copy in direct_copies(depth):
            copy.wait_send()
        for _block, _half, copies in relay_copies(depth):
            for copy in copies:
                copy.wait_send()
        return carry

    lax.fori_loop(0, plane + 1, drain, 0)
    for k in range(1, tp_count):
        pl.semaphore_signal(
            pair_ready, inc=1, device_id={"tp": (tp + k) % tp_count}, device_id_type=MESH
        )
    pl.semaphore_wait(pair_ready, tp_count - 1)
    share = out_ref.shape[1]
    copies = []
    for k in range(1, tp_count):
        other = (tp + k) % tp_count
        copies.append(
            pltpu.make_async_remote_copy(
                src_ref=att.at[pl.ds(pl.multiple_of(other * share, share), share), :],
                dst_ref=out_ref.at[tp],
                send_sem=pair_send.at[k - 1],
                recv_sem=pair_recv.at[k - 1],
                device_id={"tp": other},
                device_id_type=MESH,
            )
        )
    for copy in copies:
        copy.start()
    out_ref[tp] = att[pl.ds(pl.multiple_of(tp * share, share), share), :]
    for copy in copies:
        copy.wait()


def attended_rows(
    sp_count,
    tp_count,
    queries_narrow,
    keys_narrow,
    values_narrow,
    queries_wide,
    keys_wide,
    values_wide,
    lambda_narrow,
    lambda_wide,
    gain_narrow,
    gain_wide,
):
    planes, rows, columns = plane_shape(sp_count)
    count = queries_narrow.shape[0]
    heads_n = queries_narrow.shape[1] // (2 * DN)
    heads_w = queries_wide.shape[1] // (2 * DW)
    maps = queries_narrow.reshape(count, heads_n, 2, DN).transpose(1, 2, 0, 3)
    padded = jnp.stack(
        [
            jnp.pad(maps[:, 0], ((0, 0), (0, 0), (0, DN))),
            jnp.pad(maps[:, 1], ((0, 0), (0, 0), (DN, 0))),
        ],
        axis=1,
    )
    width = (
        keys_narrow.shape[1] + values_narrow.shape[1] + keys_wide.shape[1] + values_wide.shape[1]
    )
    per_plane = rows * columns
    features = heads_n * VN + heads_w * VW
    longest = max(rows, columns)
    tiles = 2 * (heads_n + heads_w)
    vmem = pl.BlockSpec(memory_space=pltpu.VMEM)
    smem = pl.BlockSpec(memory_space=pltpu.SMEM)
    hbm = pl.BlockSpec(memory_space=pl.ANY)
    return pl.pallas_call(
        functools.partial(attend_kernel, (planes, rows, columns, tp_count)),
        out_shape=jax.ShapeDtypeStruct((tp_count, count // tp_count, features), jnp.bfloat16),
        in_specs=[vmem, hbm, hbm, vmem, hbm, hbm, smem, smem, vmem, vmem],
        out_specs=vmem,
        scratch_shapes=[
            pltpu.VMEM((planes, per_plane, count, width), jnp.bfloat16),
            pltpu.VMEM((count, features), jnp.bfloat16),
            pltpu.VMEM((tiles, count, 128), jnp.float32),
            pltpu.VMEM((tiles, count, 128), jnp.float32),
            pltpu.VMEM((2 * heads_n, count, VN), jnp.float32),
            pltpu.VMEM((2 * heads_w, count, VW), jnp.float32),
            pltpu.SemaphoreType.DMA((4,)),
            pltpu.SemaphoreType.DMA((planes, per_plane, 2)),
            pltpu.SemaphoreType.DMA((planes, 2)),
            pltpu.SemaphoreType.DMA((planes, 2, longest)),
            pltpu.SemaphoreType.DMA((planes, 2, longest, longest)),
            pltpu.SemaphoreType.DMA((max(1, tp_count - 1),)),
            pltpu.SemaphoreType.DMA((max(1, tp_count - 1),)),
            pltpu.SemaphoreType.REGULAR,
        ],
        compiler_params=pltpu.CompilerParams(
            collective_id=0, has_side_effects=True, vmem_limit_bytes=56 * 1024 * 1024
        ),
        name="gather_attend",
    )(
        padded,
        keys_narrow,
        values_narrow,
        queries_wide,
        keys_wide,
        values_wide,
        lambda_narrow,
        lambda_wide,
        gain_narrow.reshape(1, -1),
        gain_wide.reshape(1, -1),
    )


def plane_greeting(planes, rows, columns, tp_count):
    per_plane = rows * columns
    sp = lax.axis_index("sp")
    tp = lax.axis_index("tp")
    plane = sp // per_plane
    cell = sp % per_plane
    barrier = pltpu.get_barrier_semaphore()
    for k in range(1, per_plane):
        pl.semaphore_signal(
            barrier,
            inc=1,
            device_id={"sp": plane * per_plane + (cell + k) % per_plane},
            device_id_type=MESH,
        )
    for k in range(1, planes):
        pl.semaphore_signal(
            barrier,
            inc=1,
            device_id={"sp": (plane + k) % planes * per_plane + cell},
            device_id_type=MESH,
        )
    for k in range(1, tp_count):
        pl.semaphore_signal(
            barrier, inc=1, device_id={"tp": (tp + k) % tp_count}, device_id_type=MESH
        )
    pl.semaphore_wait(barrier, per_plane - 1 + planes - 1 + tp_count - 1)
    return plane, cell, sp, tp


def dispatch_kernel(
    dims,
    group,
    normed_ref,
    slots_ref,
    inbox,
    marks,
    held,
    stage,
    load_sem,
    row_recv,
    mark_recv,
    row_send,
    mark_send,
    cell_recv,
    cell_send,
    pair_recv,
    pair_send,
):
    planes, rows, columns, tp_count = dims
    per_plane = rows * columns
    sp_now = lax.axis_index("sp")
    mine = sp_now // per_plane
    loads = [
        pltpu.make_async_copy(normed_ref, held.at[mine], load_sem.at[0]),
        pltpu.make_async_copy(slots_ref, marks.at[mine], load_sem.at[1]),
    ]
    for copy in loads:
        copy.start()
    plane, cell, sp, tp = plane_greeting(planes, rows, columns, tp_count)
    for copy in loads:
        copy.wait()
    padded = stage.shape[2]
    token_count = held.shape[1]

    def hops(source, way):
        target = {"sp": (sp + per_plane * (1 if way == 0 else planes - 1)) % (planes * per_plane)}
        return [
            pltpu.make_async_remote_copy(
                src_ref=marks.at[source],
                dst_ref=marks.at[source],
                send_sem=mark_send.at[source, way],
                recv_sem=mark_recv.at[source],
                device_id=target,
                device_id_type=MESH,
            ),
            pltpu.make_async_remote_copy(
                src_ref=held.at[source],
                dst_ref=held.at[source],
                send_sem=row_send.at[source, way],
                recv_sem=row_recv.at[source],
                device_id=target,
                device_id_type=MESH,
            ),
        ]

    def to_cell(source, k):
        other = (cell + k) % per_plane
        return pltpu.make_async_remote_copy(
            src_ref=stage.at[source, other],
            dst_ref=inbox.at[tp, source * per_plane + cell],
            send_sem=cell_send.at[source, k],
            recv_sem=cell_recv.at[source, (per_plane - k) % per_plane],
            device_id={"sp": plane * per_plane + other},
            device_id_type=MESH,
        )

    def to_pair(source, k):
        block = inbox.at[tp, pl.ds(source * per_plane, per_plane)]
        return pltpu.make_async_remote_copy(
            src_ref=block,
            dst_ref=block,
            send_sem=pair_send.at[source, k - 1],
            recv_sem=pair_recv.at[source, k - 1],
            device_id={"tp": (tp + k) % tp_count},
            device_id_type=MESH,
        )

    steps = [(0, 0)] + [(d, way) for d in range(1, planes) for way in range(2)]

    def of_step(d, way):
        source = plane - d if way == 0 else plane + d
        exists = source >= 0 if way == 0 else source < planes
        return source, exists

    def onward(source, d, way, act):
        for side in ((0, 1) if d == 0 else (way,)):

            @pl.when(plane < planes - 1 if side == 0 else plane > 0)
            def _(side=side):
                for copy in hops(source, side):
                    act(copy)

    def start(copy):
        copy.start()

    def wait_send(copy):
        copy.wait_send()

    def body(d, way):
        source, exists = of_step(d, way)

        @pl.when(exists)
        def _():
            if d > 0:
                for copy in hops(source, way):
                    copy.wait_recv()
            onward(source, d, way, start)
            tokens = held[source]
            slots = marks[source]
            row = lax.broadcasted_iota(jnp.int32, (padded, token_count), 0)
            for k in list(range(1, per_plane)) + [0]:
                other = (cell + k) % per_plane
                base = (plane * per_plane + other) * group
                wanted = jnp.where(row < group, row + base, -1).astype(jnp.float32)
                hit = slots[0:1, :] == wanted
                for choice in range(1, TOPK):
                    hit = hit | (slots[choice : choice + 1, :] == wanted)
                chosen = jnp.dot(
                    jnp.where(hit, 1.0, 0.0).astype(jnp.bfloat16),
                    tokens,
                    preferred_element_type=jnp.float32,
                ).astype(jnp.bfloat16)
                if k == 0:
                    inbox[tp, source * per_plane + cell] = chosen
                else:
                    stage[source, other] = chosen
            for k in range(1, per_plane):
                to_cell(source, k).start()

    def finish(d, way):
        source, exists = of_step(d, way)

        @pl.when(exists)
        def _():
            for k in range(1, per_plane):
                pltpu.make_async_remote_copy(
                    src_ref=stage.at[source, cell],
                    dst_ref=inbox.at[tp, source * per_plane + (cell + k) % per_plane],
                    send_sem=cell_send.at[source, k],
                    recv_sem=cell_recv.at[source, k],
                    device_id={"sp": sp},
                    device_id_type=MESH,
                ).wait_recv()
            for k in range(1, tp_count):
                to_pair(source, k).start()

    for index, step in enumerate(steps):
        body(*step)
        if index > 0:
            finish(*steps[index - 1])
    finish(*steps[-1])
    for d, way in steps:
        source, exists = of_step(d, way)

        @pl.when(exists)
        def _(source=source, d=d, way=way):
            onward(source, d, way, wait_send)
            for k in range(1, per_plane):
                to_cell(source, k).wait_send()
            for k in range(1, tp_count):
                to_pair(source, k).wait()


def dispatched_rows(dims, group, normed, slot_index, route_weights):
    planes, rows, columns, tp_count = dims
    per_plane = rows * columns
    token_count, width = normed.shape
    padded = -(-group // 16) * 16
    slots = slot_index.reshape(token_count, TOPK).astype(jnp.float32)
    slots = jnp.concatenate([slots, route_weights], axis=1).T
    hbm = pl.BlockSpec(memory_space=pl.ANY)
    dma = pltpu.SemaphoreType.DMA
    return pl.pallas_call(
        functools.partial(dispatch_kernel, dims, group),
        out_shape=[
            jax.ShapeDtypeStruct((tp_count, planes * per_plane, padded, width), jnp.bfloat16),
            jax.ShapeDtypeStruct((planes, 2 * TOPK, token_count), jnp.float32),
        ],
        in_specs=[hbm, hbm],
        out_specs=[pl.BlockSpec(memory_space=pltpu.VMEM)] * 2,
        scratch_shapes=[
            pltpu.VMEM((planes, token_count, width), jnp.bfloat16),
            pltpu.VMEM((planes, per_plane, padded, width), jnp.bfloat16),
            dma((2,)),
            dma((planes,)),
            dma((planes,)),
            dma((planes, 2)),
            dma((planes, 2)),
            dma((planes, per_plane)),
            dma((planes, per_plane)),
            dma((planes, max(1, tp_count - 1))),
            dma((planes, max(1, tp_count - 1))),
        ],
        compiler_params=pltpu.CompilerParams(
            collective_id=1, has_side_effects=True, vmem_limit_bytes=56 * 1024 * 1024
        ),
        name="dispatch",
    )(normed, slots)


def combine_kernel(
    dims,
    group,
    parts_ref,
    marks_ref,
    out_ref,
    mine,
    theirs,
    stage,
    back,
    leaving,
    landed,
    load_sem,
    pair_recv,
    pair_send,
    cell_recv,
    cell_send,
    far_recv,
    far_send,
):
    planes, rows, columns, tp_count = dims
    per_plane = rows * columns
    plane, cell, sp, tp = plane_greeting(planes, rows, columns, tp_count)
    padded = stage.shape[2]
    token_count = out_ref.shape[0]
    order = list(range(1, planes)) + [0]

    def source_of(step):
        return (plane + step) % planes

    def load(step):
        source = source_of(step)
        return pltpu.make_async_copy(
            parts_ref.at[tp, pl.ds(source * per_plane, per_plane)],
            mine.at[source],
            load_sem.at[step],
        )

    def to_pair(step, k):
        source = source_of(step)
        other = (tp + k) % tp_count
        return pltpu.make_async_remote_copy(
            src_ref=parts_ref.at[other, pl.ds(source * per_plane, per_plane)],
            dst_ref=theirs.at[k - 1, source],
            send_sem=pair_send.at[step, k - 1],
            recv_sem=pair_recv.at[step, k - 1],
            device_id={"tp": other},
            device_id_type=MESH,
        )

    def to_cell(step, k):
        source = source_of(step)
        other = (cell + k) % per_plane
        return pltpu.make_async_remote_copy(
            src_ref=stage.at[source, other],
            dst_ref=back.at[source, cell],
            send_sem=cell_send.at[step, k],
            recv_sem=cell_recv.at[step, (per_plane - k) % per_plane],
            device_id={"sp": plane * per_plane + other},
            device_id_type=MESH,
        )

    def to_far(step):
        return pltpu.make_async_remote_copy(
            src_ref=leaving.at[step],
            dst_ref=landed.at[step],
            send_sem=far_send.at[step],
            recv_sem=far_recv.at[step],
            device_id={"sp": source_of(step) * per_plane + cell},
            device_id_type=MESH,
        )

    for step in order:
        load(step).start()
        for k in range(1, tp_count):
            to_pair(step, k).start()

    def body(step):
        source = source_of(step)
        load(step).wait()
        for k in range(1, tp_count):
            to_pair(step, k).wait_recv()
        for k in list(range(1, per_plane)) + [0]:
            other = (cell + k) % per_plane
            total = mine[source, other].astype(jnp.float32)
            for i in range(tp_count - 1):
                total += theirs[i, source, other].astype(jnp.float32)
            if k == 0:
                back[source, cell] = total.astype(jnp.bfloat16)
            else:
                stage[source, other] = total.astype(jnp.bfloat16)
        for k in range(1, per_plane):
            to_cell(step, k).start()

    def finish(step):
        source = source_of(step)
        for k in range(1, per_plane):
            pltpu.make_async_remote_copy(
                src_ref=stage.at[source, cell],
                dst_ref=back.at[source, (cell + k) % per_plane],
                send_sem=cell_send.at[step, k],
                recv_sem=cell_recv.at[step, k],
                device_id={"sp": sp},
                device_id_type=MESH,
            ).wait_recv()
        marks = marks_ref[source]
        row = lax.broadcasted_iota(jnp.int32, (per_plane * padded, token_count), 0)
        block = lax.div(row, padded)
        inner = row - block * padded
        wanted = jnp.where(
            inner < group, inner + (plane * per_plane + block) * group, -1
        ).astype(jnp.float32)
        share = jnp.zeros(wanted.shape, jnp.float32)
        for choice in range(TOPK):
            share += jnp.where(
                marks[choice : choice + 1, :] == wanted,
                marks[TOPK + choice : TOPK + choice + 1, :],
                0.0,
            )
        high = share.astype(jnp.bfloat16)
        low = (share - high.astype(jnp.float32)).astype(jnp.bfloat16)
        both = jnp.concatenate([high, low], axis=1)
        for at in range(0, out_ref.shape[1], 512):
            values = back[source, :, :, at : at + 512].reshape(per_plane * padded, 512)
            pieces = lax.dot_general(
                both, values, (((0,), (0,)), ((), ())), preferred_element_type=jnp.float32
            )
            total = pieces[:token_count] + pieces[token_count:]
            if step == 0:
                out_ref[:, at : at + 512] = total
            else:
                leaving[step, :, at : at + 512] = total.astype(jnp.bfloat16)
        if step > 0:
            to_far(step).start()

    for index, step in enumerate(order):
        body(step)
        if index > 0:
            finish(order[index - 1])
    finish(order[-1])
    for step in range(1, planes):
        to_far(step).wait_recv()
        out_ref[...] += landed[step].astype(jnp.float32)
    for step in order:
        for k in range(1, tp_count):
            to_pair(step, k).wait_send()
        for k in range(1, per_plane):
            to_cell(step, k).wait_send()
        if step > 0:
            to_far(step).wait_send()


def combined_rows(dims, group, parts, marks):
    planes, rows, columns, tp_count = dims
    per_plane = rows * columns
    padded, width = parts.shape[2:]
    token_count = marks.shape[2]
    dma = pltpu.SemaphoreType.DMA
    block = (planes, per_plane, padded, width)
    pairs = max(1, tp_count - 1)
    return pl.pallas_call(
        functools.partial(combine_kernel, dims, group),
        out_shape=jax.ShapeDtypeStruct((token_count, width), jnp.float32),
        in_specs=[pl.BlockSpec(memory_space=pl.ANY), pl.BlockSpec(memory_space=pltpu.VMEM)],
        out_specs=pl.BlockSpec(memory_space=pltpu.VMEM),
        scratch_shapes=[
            pltpu.VMEM(block, jnp.bfloat16),
            pltpu.VMEM((pairs,) + block, jnp.bfloat16),
            pltpu.VMEM(block, jnp.bfloat16),
            pltpu.VMEM(block, jnp.bfloat16),
            pltpu.VMEM((planes, token_count, width), jnp.bfloat16),
            pltpu.VMEM((planes, token_count, width), jnp.bfloat16),
            dma((planes,)),
            dma((planes, pairs)),
            dma((planes, pairs)),
            dma((planes, per_plane)),
            dma((planes, per_plane)),
            dma((planes,)),
            dma((planes,)),
        ],
        compiler_params=pltpu.CompilerParams(
            collective_id=2, has_side_effects=True, vmem_limit_bytes=56 * 1024 * 1024
        ),
        name="combine",
    )(parts, marks)


def run_experts(incoming, expert_gate, expert_up, expert_down, capacity):
    sources = incoming.shape[0]
    local_experts = expert_gate.shape[0]
    grouped = incoming.reshape(sources, local_experts, capacity, D)
    gate_part = jnp.einsum(
        "rjcd,jdf->rjcf", grouped, expert_gate, preferred_element_type=jnp.float32
    )
    up_part = jnp.einsum("rjcd,jdf->rjcf", grouped, expert_up, preferred_element_type=jnp.float32)
    hidden = (jax.nn.silu(gate_part) * up_part).astype(jnp.bfloat16)
    result = jnp.stack(
        [
            jnp.einsum(
                "rcf,fd->rcd", hidden[:, j], expert_down[j], preferred_element_type=jnp.float32
            ).astype(jnp.bfloat16)
            for j in range(local_experts)
        ],
        axis=1,
    )
    return result.reshape(sources, local_experts * capacity, D)


def shards(
    queries_narrow,
    keys_narrow,
    values_narrow,
    queries_wide,
    keys_wide,
    values_wide,
    lambda_narrow,
    lambda_wide,
    gain_narrow,
    gain_wide,
    out_narrow,
    out_wide,
    stream,
    gain_mix,
    gain_ffn,
    gain_post,
    shared_gate,
    shared_up,
    shared_down,
    expert_gate,
    expert_up,
    expert_down,
    expert_ids,
    route_weights,
):
    sp_count = lax.axis_size("sp")
    attended = attended_rows(
        sp_count,
        lax.axis_size("tp"),
        queries_narrow,
        keys_narrow,
        values_narrow,
        queries_wide,
        keys_wide,
        values_wide,
        lambda_narrow,
        lambda_wide,
        gain_narrow,
        gain_wide,
    )
    narrow_width = out_narrow.shape[0] // attended.shape[0]
    attended = attended.transpose(1, 0, 2)
    narrow_rows = attended[:, :, :narrow_width].reshape(attended.shape[0], -1)
    wide_rows = attended[:, :, narrow_width:].reshape(attended.shape[0], -1)
    projected = jnp.dot(narrow_rows, out_narrow, preferred_element_type=jnp.float32) + jnp.dot(
        wide_rows, out_wide, preferred_element_type=jnp.float32
    )
    mixed_rows = (stream.astype(jnp.float32) + rms_scale(projected, gain_mix)).astype(jnp.bfloat16)
    normed = rms_scale(mixed_rows.astype(jnp.float32), gain_ffn).astype(jnp.bfloat16)
    row_count = normed.shape[0]
    tp_count = lax.axis_size("tp")
    local_experts = expert_gate.shape[0]
    experts_all = local_experts * sp_count
    capacity = max(2, 3 * row_count * TOPK // (2 * experts_all))
    flat_ids = expert_ids.reshape(-1)
    onehot = (flat_ids[:, None] == jnp.arange(experts_all, dtype=jnp.int32)[None, :]).astype(
        jnp.int32
    )
    earlier = jnp.cumsum(onehot, axis=0) - onehot
    slot_rank = jnp.sum(earlier * onehot, axis=1)
    slot_index = flat_ids * capacity + slot_rank
    group = local_experts * capacity
    dims = plane_shape(sp_count) + (tp_count,)
    all_rows, marks = dispatched_rows(dims, group, normed, slot_index, route_weights)
    padded = all_rows.shape[2]
    partials = run_experts(
        all_rows[:, :, :group].reshape(tp_count * sp_count, group, D),
        expert_gate,
        expert_up,
        expert_down,
        capacity,
    )
    partials = partials.astype(jnp.bfloat16).reshape(tp_count, sp_count, group, D)
    if padded > group:
        partials = jnp.pad(partials, ((0, 0), (0, 0), (0, padded - group), (0, 0)))
    routed = combined_rows(dims, group, partials, marks)
    shared_hidden = (
        jax.nn.silu(jnp.dot(normed, shared_gate, preferred_element_type=jnp.float32))
        * jnp.dot(normed, shared_up, preferred_element_type=jnp.float32)
    ).astype(jnp.bfloat16)
    shared_out = jnp.dot(shared_hidden, shared_down, preferred_element_type=jnp.float32)
    combined = shared_out + routed
    return (mixed_rows.astype(jnp.float32) + rms_scale(combined, gain_post)).astype(jnp.bfloat16)


def solution(mesh):
    return jax.shard_map(
        shards,
        mesh=mesh,
        in_specs=(
            P("sp", "tp"),
            P("sp", "tp"),
            P("sp", "tp"),
            P("sp", "tp"),
            P("sp", "tp"),
            P("sp", "tp"),
            P("tp"),
            P("tp"),
            P(),
            P(),
            P(),
            P(),
            P(("sp", "tp"), None),
            P(),
            P(),
            P(),
            P(),
            P(),
            P(),
            P("sp", None, "tp"),
            P("sp", None, "tp"),
            P("sp", "tp", None),
            P(("sp", "tp"), None),
            P(("sp", "tp"), None),
        ),
        out_specs=P(("sp", "tp"), None),
        check_vma=False,
    )
```

profile of v0, /device:TPU:9, one launch (start us, length us, event | category | flops | bytes accessed | tf_op | source)
XLA Modules:
  0.0 239.1 jit_solution(8839516690784269144)
XLA Ops:
  0.0 1.2 copy.29
  1.2 0.3 copy.30
  1.6 0.2 pad_bitcast_fusion
  1.7 0.8 pad_maximum_fusion.1.qn_ref
  2.6 48.0 %gather_attend.1 = bf16[2,128,1024]{2,1,0:T(8,128)(2,1)} custom-call(bf16[4,2,256,128]{3,2,1,0:T(8,128)(2,1)} %pad_maximum_fusion.1.qn_ref, bf16[256,128]{1,0:T(8,128)(2,1)} %kn_ref.1, bf16[256,128]{1,0:T(8,128)(2,1)} %vn_ref.1, bf16[256,512]{1,0:T(8,128)(2,1)} %qw_ref.1, bf16[256,256]{1,0:T(8,128)(2,1)} %kw_ref.1, bf16[256,256]{1,0:T(8,128)(2,1)} %vw_ref.1, ...), custom_call_target="tpu_custom_call" | custom-call | tf_op jit(solution)/shard_map/gather_attend/pallas_call | solution.py:440
  50.6 1.1 fusion.36
  51.6 0.8 copy.32
  52.5 3.0 %fusion.37 = f32[128,2048]{1,0:T(8,128)S(1)} fusion(bf16[128,1024]{0,1:T(8,128)(2,1)} %bitcast.101, bf16[1024,2048]{1,0:T(8,128)(2,1)} %param.34), kind=kOutput, calls=%fused_computation.65 | convolution fusion | flops 536870912 | bytes 5505024 | tf_op jit(solution)/shard_map/dot_general | solution.py:962
  55.5 0.8 copy.33
  56.4 3.1 %multiply_reduce_fusion.1 = (f32[128]{0:T(128)S(1)}, f32[128,2048]{1,0:T(8,128)S(1)}) fusion(f32[128,2048]{1,0:T(8,128)S(1)} %fusion.37, bf16[128,1024]{0,1:T(8,128)(2,1)} %bitcast.100, bf16[1024,2048]{1,0:T(8,128)(2,1)} %param.35), kind=kOutput, calls=%fused_computation.35 | convolution fusion | flops 537657216 | bytes 6554112 | tf_op jit(solution)/shard_map/dot_general | solution.py:962
  59.6 0.4 fusion.17
  59.9 0.3 copy-done.6
  60.2 1.0 fusion.19.normed_ref
  61.2 0.1 copy.34
  61.3 0.1 eq.29
  61.4 1.2 reduce-window.6
  62.6 0.2 slice_reduce_fusion
  62.9 0.1 eq.25
  63.1 0.1 reduce_sum.41
  63.3 0.6 maximum_bitcast_fusion.slots_ref
  63.9 77.5 %dispatch.1 = (bf16[2,16,48,2048]{3,2,1,0:T(8,128)(2,1)}, f32[4,8,128]{2,1,0:T(8,128)}) custom-call(bf16[128,2048]{1,0:T(8,128)(2,1)} %fusion.19.normed_ref, f32[8,128]{1,0:T(8,128)} %maximum_bitcast_fusion.slots_ref), custom_call_target="tpu_custom_call" | custom-call | tf_op jit(solution)/shard_map/dispatch/pallas_call | solution.py:681
  141.4 4.7 %fusion.2 = f32[2,32,24,256]{3,2,1,0:T(8,128)S(1)} fusion(bf16[32,2,24,2048]{3,2,1,0:T(8,128)(2,1)} %bitcast.104, bf16[2,2048,256]{2,1,0:T(8,128)(2,1)S(1)} %copy-done), kind=kOutput, calls=%fused_computation.3 | convolution fusion | flops 1610612736 | bytes 9961472 | tf_op jit(solution)/shard_map/rjcd,jdf->rjcf/dot_general | solution.py:900
  146.2 0.4 copy-done.11
  146.7 2.2 fusion.8
  148.8 1.0 fusion.4
  149.8 1.0 fusion.5
  150.8 0.6 pad_maximum_fusion
  151.4 3.2 %copy.40 = bf16[32,2,24,2048]{3,2,1,0:T(8,128)(2,1)} copy(bf16[32,2,24,2048]{3,2,0,1:T(8,128)(2,1)S(1)} %pad_maximum_fusion) | data formatting | bytes 12582912 | tf_op jit(solution)/shard_map/stack | solution.py:905
  154.7 77.4 %combine.1 = f32[128,2048]{1,0:T(8,128)} custom-call(bf16[2,16,48,2048]{3,2,1,0:T(8,128)(2,1)} %bitcast.96, f32[4,8,128]{2,1,0:T(8,128)} %get-tuple-element.8.marks_ref), custom_call_target="tpu_custom_call" | custom-call | tf_op jit(solution)/shard_map/combine/pallas_call | solution.py:869
  232.0 0.5 fusion.38
  232.5 4.4 %multiply_reduce_fusion = (f32[128]{0:T(128)S(1)}, f32[128,2048]{1,0:T(8,128)}) fusion(f32[128,2048]{1,0:T(8,128)} %combine.1, bf16[512,2048]{1,0:T(8,128)(2,1)} %param.42, bf16[128,2048]{1,0:T(8,128)(2,1)S(1)} %copy-done.1, bf16[2048,512]{1,0:T(8,128)(2,1)} %param.41, f32[128,512]{1,0:T(8,128)S(1)} %fusion.38), kind=kOutput, calls=%fused_computation.31 | convolution fusion | flops 538050432 | bytes 7078400 | tf_op jit(solution)/shard_map/dot_general | solution.py:998
  236.9 2.2 fusion.20
  (32 shorter events, 0.3 us)
Async XLA Ops:
  0.0 141.4 %copy-start = (bf16[2,2048,256]{2,1,0:T(8,128)(2,1)S(1)}, bf16[2,2048,256]{2,1,0:T(8,128)(2,1)}, u32[]{:S(2)}) copy-start(bf16[2,2048,256]{2,1,0:T(8,128)(2,1)} %param.43) | copy-start | bytes 6291460
  56.3 3.2 %copy-start.4 = (bf16[128,2048]{1,0:T(8,128)(2,1)S(1)}, bf16[128,2048]{1,0:T(8,128)(2,1)}, u32[]{:S(2)}) copy-start(bf16[128,2048]{1,0:T(8,128)(2,1)} %param.36) | copy-start | bytes 1572868
  56.4 3.2 %copy-start.5 = (f32[2048]{0:T(1024)S(1)}, f32[2048]{0:T(1024)}, u32[]{:S(2)}) copy-start(f32[2048]{0:T(1024)} %param.37) | copy-start | bytes 24580
  59.5 0.7 copy-start.6
  59.5 1.7 copy-start.8
  59.5 3.7 %copy-start.9 = (f32[128,4]{0,1:T(4,128)S(1)}, f32[128,4]{0,1:T(4,128)}, u32[]{:S(2)}) copy-start(f32[128,4]{0,1:T(4,128)} %param.47) | copy-start | bytes 6148
  141.4 4.8 %copy-start.10 = (bf16[2,16,48,2048]{3,2,1,0:T(8,128)(2,1)S(1)}, bf16[2,16,48,2048]{3,2,1,0:T(8,128)(2,1)}, u32[]{:S(2)}) copy-start(bf16[2,16,48,2048]{3,2,1,0:T(8,128)(2,1)} %get-tuple-element.7) | copy-start | bytes 18874372
  141.4 5.2 %copy-start.11 = (bf16[2,2048,256]{2,1,0:T(8,128)(2,1)S(1)}, bf16[2,2048,256]{2,1,0:T(8,128)(2,1)}, u32[]{:S(2)}) copy-start(bf16[2,2048,256]{2,1,0:T(8,128)(2,1)} %param.44) | copy-start | bytes 6291460
  146.6 2.2 copy-start.3
  154.6 77.4 %copy-start.1 = (bf16[128,2048]{1,0:T(8,128)(2,1)S(1)}, bf16[128,2048]{1,0:T(8,128)(2,1)}, u32[]{:S(2)}) copy-start(bf16[128,2048]{1,0:T(8,128)(2,1)} %fusion.19.normed_ref) | copy-start | bytes 1572868
  154.7 77.4 %copy-start.2 = (bf16[2048,512]{1,0:T(8,128)(2,1)S(1)}, bf16[2048,512]{1,0:T(8,128)(2,1)}, u32[]{:S(2)}) copy-start(bf16[2048,512]{1,0:T(8,128)(2,1)} %param.40) | copy-start | bytes 6291460
  232.5 4.4 %copy-start.7 = (f32[2048]{0:T(1024)S(1)}, f32[2048]{0:T(1024)}, u32[]{:S(2)}) copy-start(f32[2048]{0:T(1024)} %param.39) | copy-start | bytes 24580
where the time goes:
time: 239 us
  Pallas kernels  203 us (85%)
  matrix products  19.9 us (8%)
  local copies, waits for them, and re-layouts  9.16 us (4%)
  other arithmetic  6.99 us (3%)
    pallas_call x1, Pallas kernels, dispatched_rows(): pl.pallas_call(functools.partial(dispatch_kernel, dims, group), out_shape...  77.5 us
    pallas_call x1, Pallas kernels, combined_rows(): pl.pallas_call(functools.partial(combine_kernel, dims, group), out_shape=...  77.4 us
    pallas_call x1, Pallas kernels, attended_rows(): pl.pallas_call(functools.partial(attend_kernel, (planes, rows, columns, t...  48 us

commit v1 on v0

--- a/solution.py
+++ b/solution.py
@@ -709,6 +709,7 @@
 def combine_kernel(
     dims,
     group,
+    chunks,
     parts_ref,
     marks_ref,
     out_ref,
@@ -731,86 +732,92 @@
     plane, cell, sp, tp = plane_greeting(planes, rows, columns, tp_count)
     padded = stage.shape[2]
     token_count = out_ref.shape[0]
-    order = list(range(1, planes)) + [0]
-
-    def source_of(step):
-        return (plane + step) % planes
-
-    def load(step):
-        source = source_of(step)
+
+    order = []
+    low, high = jnp.int32(0), jnp.int32(planes - 1)
+    for _ in range(planes - 1):
+        use_high = high - plane >= plane - low
+        order.append(jnp.where(use_high, high, low))
+        high = jnp.where(use_high, high - 1, high)
+        low = jnp.where(use_high, low, low + 1)
+    order.append(plane)
+
+    wide = out_ref.shape[1] // chunks
+
+    def span(chunk):
+        return pl.ds(chunk * wide, wide)
+
+    def load(source, chunk):
         return pltpu.make_async_copy(
-            parts_ref.at[tp, pl.ds(source * per_plane, per_plane)],
-            mine.at[source],
-            load_sem.at[step],
-        )
-
-    def to_pair(step, k):
-        source = source_of(step)
+            parts_ref.at[tp, pl.ds(source * per_plane, per_plane), :, span(chunk)],
+            mine.at[source, :, :, span(chunk)],
+            load_sem.at[source, chunk],
+        )
+
+    def to_pair(source, chunk, k):
         other = (tp + k) % tp_count
         return pltpu.make_async_remote_copy(
-            src_ref=parts_ref.at[other, pl.ds(source * per_plane, per_plane)],
-            dst_ref=theirs.at[k - 1, source],
-            send_sem=pair_send.at[step, k - 1],
-            recv_sem=pair_recv.at[step, k - 1],
+            src_ref=parts_ref.at[other, pl.ds(source * per_plane, per_plane), :, span(chunk)],
+            dst_ref=theirs.at[k - 1, source, :, :, span(chunk)],
+            send_sem=pair_send.at[source, chunk, k - 1],
+            recv_sem=pair_recv.at[source, chunk, k - 1],
             device_id={"tp": other},
             device_id_type=MESH,
         )
 
-    def to_cell(step, k):
-        source = source_of(step)
+    def to_cell(source, chunk, k):
         other = (cell + k) % per_plane
         return pltpu.make_async_remote_copy(
-            src_ref=stage.at[source, other],
-            dst_ref=back.at[source, cell],
-            send_sem=cell_send.at[step, k],
-            recv_sem=cell_recv.at[step, (per_plane - k) % per_plane],
+            src_ref=stage.at[source, other, :, span(chunk)],
+            dst_ref=back.at[source, cell, :, span(chunk)],
+            send_sem=cell_send.at[source, chunk, k],
+            recv_sem=cell_recv.at[source, chunk, (per_plane - k) % per_plane],
             device_id={"sp": plane * per_plane + other},
             device_id_type=MESH,
         )
 
-    def to_far(step):
+    def from_cell(source, chunk, k):
         return pltpu.make_async_remote_copy(
-            src_ref=leaving.at[step],
-            dst_ref=landed.at[step],
-            send_sem=far_send.at[step],
-            recv_sem=far_recv.at[step],
-            device_id={"sp": source_of(step) * per_plane + cell},
+            src_ref=stage.at[source, cell, :, span(chunk)],
+            dst_ref=back.at[source, (cell + k) % per_plane, :, span(chunk)],
+            send_sem=cell_send.at[source, chunk, k],
+            recv_sem=cell_recv.at[source, chunk, k],
+            device_id={"sp": sp},
             device_id_type=MESH,
         )
 
-    for step in order:
-        load(step).start()
+    def onward(source, chunk, way, target):
+        return pltpu.make_async_remote_copy(
+            src_ref=leaving.at[source, :, span(chunk)],
+            dst_ref=landed.at[way, source, :, span(chunk)],
+            send_sem=far_send.at[source, chunk],
+            recv_sem=far_recv.at[way, source, chunk],
+            device_id={"sp": target},
+            device_id_type=MESH,
+        )
+
+    items = [(source, chunk) for source in order for chunk in range(chunks)]
+    for item in items:
+        load(*item).start()
         for k in range(1, tp_count):
-            to_pair(step, k).start()
-
-    def body(step):
-        source = source_of(step)
-        load(step).wait()
+            to_pair(*item, k).start()
+
+    def body(source, chunk):
+        load(source, chunk).wait()
         for k in range(1, tp_count):
-            to_pair(step, k).wait_recv()
+            to_pair(source, chunk, k).wait_recv()
         for k in list(range(1, per_plane)) + [0]:
             other = (cell + k) % per_plane
-            total = mine[source, other].astype(jnp.float32)
+            total = mine[source, other, :, span(chunk)].astype(jnp.float32)
             for i in range(tp_count - 1):
-                total += theirs[i, source, other].astype(jnp.float32)
+                total += theirs[i, source, other, :, span(chunk)].astype(jnp.float32)
             if k == 0:
-                back[source, cell] = total.astype(jnp.bfloat16)
+                back[source, cell, :, span(chunk)] = total.astype(jnp.bfloat16)
             else:
-                stage[source, other] = total.astype(jnp.bfloat16)
-        for k in range(1, per_plane):
-            to_cell(step, k).start()
-
-    def finish(step):
-        source = source_of(step)
-        for k in range(1, per_plane):
-            pltpu.make_async_remote_copy(
-                src_ref=stage.at[source, cell],
-                dst_ref=back.at[source, (cell + k) % per_plane],
-                send_sem=cell_send.at[step, k],
-                recv_sem=cell_recv.at[step, k],
-                device_id={"sp": sp},
-                device_id_type=MESH,
-            ).wait_recv()
+                stage[source, other, :, span(chunk)] = total.astype(jnp.bfloat16)
+                to_cell(source, chunk, k).start()
+
+    def shares(source):
         marks = marks_ref[source]
         row = lax.broadcasted_iota(jnp.int32, (per_plane * padded, token_count), 0)
         block = lax.div(row, padded)
@@ -827,35 +834,58 @@
             )
         high = share.astype(jnp.bfloat16)
         low = (share - high.astype(jnp.float32)).astype(jnp.bfloat16)
-        both = jnp.concatenate([high, low], axis=1)
-        for at in range(0, out_ref.shape[1], 512):
+        return jnp.concatenate([high, low], axis=1)
+
+    def finish(source, chunk, both, last):
+        for k in range(1, per_plane):
+            from_cell(source, chunk, k).wait_recv()
+        begin = chunk * wide
+        for at in range(begin, begin + wide, 512):
             values = back[source, :, :, at : at + 512].reshape(per_plane * padded, 512)
             pieces = lax.dot_general(
                 both, values, (((0,), (0,)), ((), ())), preferred_element_type=jnp.float32
             )
-            total = pieces[:token_count] + pieces[token_count:]
-            if step == 0:
-                out_ref[:, at : at + 512] = total
-            else:
-                leaving[step, :, at : at + 512] = total.astype(jnp.bfloat16)
-        if step > 0:
-            to_far(step).start()
-
-    for index, step in enumerate(order):
-        body(step)
-        if index > 0:
-            finish(order[index - 1])
-    finish(order[-1])
-    for step in range(1, planes):
-        to_far(step).wait_recv()
-        out_ref[...] += landed[step].astype(jnp.float32)
-    for step in order:
-        for k in range(1, tp_count):
-            to_pair(step, k).wait_send()
-        for k in range(1, per_plane):
-            to_cell(step, k).wait_send()
-        if step > 0:
-            to_far(step).wait_send()
+            out_ref[:, at : at + 512] = pieces[:token_count] + pieces[token_count:]
+        if last:
+            comes = [(0, plane > 0), (1, plane < planes - 1)]
+        else:
+            up = source > plane
+            comes = [
+                (0, up & (plane > 0)),
+                (1, jnp.logical_not(up) & (plane < planes - 1)),
+            ]
+        for way, exists in comes:
+
+            @pl.when(exists)
+            def _(way=way):
+                onward(source, chunk, way, sp).wait_recv()
+                out_ref[:, span(chunk)] += landed[way, source, :, span(chunk)].astype(jnp.float32)
+
+        if not last:
+            leaving[source, :, span(chunk)] = out_ref[:, span(chunk)].astype(jnp.bfloat16)
+
+            @pl.when(up)
+            def _():
+                onward(source, chunk, 0, sp + per_plane).start()
+
+            @pl.when(jnp.logical_not(up))
+            def _():
+                onward(source, chunk, 1, sp - per_plane).start()
+
+    for item in items:
+        body(*item)
+    for index, source in enumerate(order):
+        both = shares(source)
+        for chunk in range(chunks):
+            finish(source, chunk, both, index == planes - 1)
+    for index, source in enumerate(order):
+        for chunk in range(chunks):
+            for k in range(1, tp_count):
+                to_pair(source, chunk, k).wait_send()
+            for k in range(1, per_plane):
+                to_cell(source, chunk, k).wait_send()
+            if index < planes - 1:
+                onward(source, chunk, 0, sp).wait_send()
 
 
 def combined_rows(dims, group, parts, marks):
@@ -866,8 +896,9 @@
     dma = pltpu.SemaphoreType.DMA
     block = (planes, per_plane, padded, width)
     pairs = max(1, tp_count - 1)
+    chunks = math.gcd(width // 512, 2)
     return pl.pallas_call(
-        functools.partial(combine_kernel, dims, group),
+        functools.partial(combine_kernel, dims, group, chunks),
         out_shape=jax.ShapeDtypeStruct((token_count, width), jnp.float32),
         in_specs=[pl.BlockSpec(memory_space=pl.ANY), pl.BlockSpec(memory_space=pltpu.VMEM)],
         out_specs=pl.BlockSpec(memory_space=pltpu.VMEM),
@@ -877,14 +908,14 @@
             pltpu.VMEM(block, jnp.bfloat16),
             pltpu.VMEM(block, jnp.bfloat16),
             pltpu.VMEM((planes, token_count, width), jnp.bfloat16),
-            pltpu.VMEM((planes, token_count, width), jnp.bfloat16),
-            dma((planes,)),
-            dma((planes, pairs)),
-            dma((planes, pairs)),
-            dma((planes, per_plane)),
-            dma((planes, per_plane)),
-            dma((planes,)),
-            dma((planes,)),
+            pltpu.VMEM((2, planes, token_count, width), jnp.bfloat16),
+            dma((planes, chunks)),
+            dma((planes, chunks, pairs)),
+            dma((planes, chunks, pairs)),
+            dma((planes, chunks, per_plane)),
+            dma((planes, chunks, per_plane)),
+            dma((2, planes, chunks)),
+            dma((planes, chunks)),
         ],
         compiler_params=pltpu.CompilerParams(
             collective_id=2, has_side_effects=True, vmem_limit_bytes=56 * 1024 * 1024

time: 239 us -> 227 us (0.950)
  the two profiles are of different devices: /device:TPU:9 before, /device:TPU:0 now
where the time goes in v1:
time: 227 us; the launch traced here: 226 us
  Pallas kernels  190 us (84%)
  matrix products  19.9 us (9%)
  local copies, waits for them, and re-layouts  9.16 us (4%)
  other arithmetic  6.99 us (3%)
    pallas_call x1, Pallas kernels, dispatched_rows(): pl.pallas_call(functools.partial(dispatch_kernel, dims, group), out_shape...  104 us
    pallas_call x1, Pallas kernels, combined_rows(): pl.pallas_call(functools.partial(combine_kernel, dims, group, chunks), ou...  51.9 us
    pallas_call x1, Pallas kernels, attended_rows(): pl.pallas_call(functools.partial(attend_kernel, (planes, rows, columns, t...  34.6 us
    dot_general x1, matrix products, run_experts(): jnp.einsum('rjcd,jdf->rjcf', grouped, expert_gate, preferred_element_type...  4.75 us

profile of v1, /device:TPU:0, one launch (start us, length us, event | category | flops | bytes accessed | tf_op | source)
XLA Modules:
  0.0 226.5 jit_solution(3163333238222683636)
XLA Ops:
  0.0 1.2 copy.29
  1.2 0.3 copy.30
  1.6 0.2 pad_bitcast_fusion
  1.7 0.8 pad_maximum_fusion.1.qn_ref
  2.6 34.6 %gather_attend.1 = bf16[2,128,1024]{2,1,0:T(8,128)(2,1)} custom-call(bf16[4,2,256,128]{3,2,1,0:T(8,128)(2,1)} %pad_maximum_fusion.1.qn_ref, bf16[256,128]{1,0:T(8,128)(2,1)} %kn_ref.1, bf16[256,128]{1,0:T(8,128)(2,1)} %vn_ref.1, bf16[256,512]{1,0:T(8,128)(2,1)} %qw_ref.1, bf16[256,256]{1,0:T(8,128)(2,1)} %kw_ref.1, bf16[256,256]{1,0:T(8,128)(2,1)} %vw_ref.1, ...), custom_call_target="tpu_custom_call" | custom-call | tf_op jit(solution)/shard_map/gather_attend/pallas_call | solution.py:440
  37.2 1.1 fusion.36
  38.3 0.8 copy.32
  39.1 3.0 %fusion.37 = f32[128,2048]{1,0:T(8,128)S(1)} fusion(bf16[128,1024]{0,1:T(8,128)(2,1)} %bitcast.101, bf16[1024,2048]{1,0:T(8,128)(2,1)} %param.34), kind=kOutput, calls=%fused_computation.65 | convolution fusion | flops 536870912 | bytes 5505024 | tf_op jit(solution)/shard_map/dot_general | solution.py:993
  42.1 0.8 copy.33
  43.0 3.1 %multiply_reduce_fusion.1 = (f32[128]{0:T(128)S(1)}, f32[128,2048]{1,0:T(8,128)S(1)}) fusion(f32[128,2048]{1,0:T(8,128)S(1)} %fusion.37, bf16[128,1024]{0,1:T(8,128)(2,1)} %bitcast.100, bf16[1024,2048]{1,0:T(8,128)(2,1)} %param.35), kind=kOutput, calls=%fused_computation.35 | convolution fusion | flops 537657216 | bytes 6554112 | tf_op jit(solution)/shard_map/dot_general | solution.py:993
  46.2 0.4 fusion.17
  46.6 0.3 copy-done.6
  46.8 1.0 fusion.19.normed_ref
  47.8 0.1 copy.34
  47.9 0.1 eq.29
  48.0 1.2 reduce-window.6
  49.2 0.2 slice_reduce_fusion
  49.5 0.1 eq.25
  49.7 0.1 reduce_sum.41
  49.9 0.6 maximum_bitcast_fusion.slots_ref
  50.5 103.7 %dispatch.1 = (bf16[2,16,48,2048]{3,2,1,0:T(8,128)(2,1)}, f32[4,8,128]{2,1,0:T(8,128)}) custom-call(bf16[128,2048]{1,0:T(8,128)(2,1)} %fusion.19.normed_ref, f32[8,128]{1,0:T(8,128)} %maximum_bitcast_fusion.slots_ref), custom_call_target="tpu_custom_call" | custom-call | tf_op jit(solution)/shard_map/dispatch/pallas_call | solution.py:681
  154.3 4.8 %fusion.2 = f32[2,32,24,256]{3,2,1,0:T(8,128)S(1)} fusion(bf16[32,2,24,2048]{3,2,1,0:T(8,128)(2,1)} %bitcast.104, bf16[2,2048,256]{2,1,0:T(8,128)(2,1)S(1)} %copy-done), kind=kOutput, calls=%fused_computation.3 | convolution fusion | flops 1610612736 | bytes 9961472 | tf_op jit(solution)/shard_map/rjcd,jdf->rjcf/dot_general | solution.py:931
  159.0 0.4 copy-done.11
  159.5 2.2 fusion.8
  161.6 1.0 fusion.4
  162.6 1.0 fusion.5
  163.6 0.6 pad_maximum_fusion
  164.2 3.2 %copy.40 = bf16[32,2,24,2048]{3,2,1,0:T(8,128)(2,1)} copy(bf16[32,2,24,2048]{3,2,0,1:T(8,128)(2,1)S(1)} %pad_maximum_fusion) | data formatting | bytes 12582912 | tf_op jit(solution)/shard_map/stack | solution.py:936
  167.5 51.9 %combine.1 = f32[128,2048]{1,0:T(8,128)} custom-call(bf16[2,16,48,2048]{3,2,1,0:T(8,128)(2,1)} %bitcast.96, f32[4,8,128]{2,1,0:T(8,128)} %get-tuple-element.8.marks_ref), custom_call_target="tpu_custom_call" | custom-call | tf_op jit(solution)/shard_map/combine/pallas_call | solution.py:900
  219.4 0.4 fusion.38
  219.9 4.4 %multiply_reduce_fusion = (f32[128]{0:T(128)S(1)}, f32[128,2048]{1,0:T(8,128)}) fusion(f32[128,2048]{1,0:T(8,128)} %combine.1, bf16[512,2048]{1,0:T(8,128)(2,1)} %param.42, bf16[128,2048]{1,0:T(8,128)(2,1)S(1)} %copy-done.1, bf16[2048,512]{1,0:T(8,128)(2,1)} %param.41, f32[128,512]{1,0:T(8,128)S(1)} %fusion.38), kind=kOutput, calls=%fused_computation.31 | convolution fusion | flops 538050432 | bytes 7078400 | tf_op jit(solution)/shard_map/dot_general | solution.py:1029
  224.2 2.2 fusion.20
  (32 shorter events, 0.3 us)
Async XLA Ops:
  0.0 154.2 %copy-start = (bf16[2,2048,256]{2,1,0:T(8,128)(2,1)S(1)}, bf16[2,2048,256]{2,1,0:T(8,128)(2,1)}, u32[]{:S(2)}) copy-start(bf16[2,2048,256]{2,1,0:T(8,128)(2,1)} %param.43) | copy-start | bytes 6291460
  43.0 3.2 %copy-start.4 = (bf16[128,2048]{1,0:T(8,128)(2,1)S(1)}, bf16[128,2048]{1,0:T(8,128)(2,1)}, u32[]{:S(2)}) copy-start(bf16[128,2048]{1,0:T(8,128)(2,1)} %param.36) | copy-start | bytes 1572868
  43.0 3.2 %copy-start.5 = (f32[2048]{0:T(1024)S(1)}, f32[2048]{0:T(1024)}, u32[]{:S(2)}) copy-start(f32[2048]{0:T(1024)} %param.37) | copy-start | bytes 24580
  46.1 0.7 copy-start.6
  46.1 1.7 copy-start.8
  46.1 3.7 %copy-start.9 = (f32[128,4]{0,1:T(4,128)S(1)}, f32[128,4]{0,1:T(4,128)}, u32[]{:S(2)}) copy-start(f32[128,4]{0,1:T(4,128)} %param.47) | copy-start | bytes 6148
  154.2 4.8 %copy-start.10 = (bf16[2,16,48,2048]{3,2,1,0:T(8,128)(2,1)S(1)}, bf16[2,16,48,2048]{3,2,1,0:T(8,128)(2,1)}, u32[]{:S(2)}) copy-start(bf16[2,16,48,2048]{3,2,1,0:T(8,128)(2,1)} %get-tuple-element.7) | copy-start | bytes 18874372
  154.2 5.2 %copy-start.11 = (bf16[2,2048,256]{2,1,0:T(8,128)(2,1)S(1)}, bf16[2,2048,256]{2,1,0:T(8,128)(2,1)}, u32[]{:S(2)}) copy-start(bf16[2,2048,256]{2,1,0:T(8,128)(2,1)} %param.44) | copy-start | bytes 6291460
  159.5 2.2 copy-start.3
  167.5 51.9 %copy-start.1 = (bf16[128,2048]{1,0:T(8,128)(2,1)S(1)}, bf16[128,2048]{1,0:T(8,128)(2,1)}, u32[]{:S(2)}) copy-start(bf16[128,2048]{1,0:T(8,128)(2,1)} %fusion.19.normed_ref) | copy-start | bytes 1572868
  167.5 51.9 %copy-start.2 = (bf16[2048,512]{1,0:T(8,128)(2,1)S(1)}, bf16[2048,512]{1,0:T(8,128)(2,1)}, u32[]{:S(2)}) copy-start(bf16[2048,512]{1,0:T(8,128)(2,1)} %param.40) | copy-start | bytes 6291460
  219.9 4.4 %copy-start.7 = (f32[2048]{0:T(1024)S(1)}, f32[2048]{0:T(1024)}, u32[]{:S(2)}) copy-start(f32[2048]{0:T(1024)} %param.39) | copy-start | bytes 24580

commit v2 on v1

--- a/solution.py
+++ b/solution.py
@@ -45,189 +45,259 @@
     qw_ref,
     kw_ref,
     vw_ref,
-    lamn_ref,
-    lamw_ref,
+    lam_ref,
     gainn_ref,
     gainw_ref,
-    out_ref,
+    outn_ref,
+    outw_ref,
     kv,
-    att,
+    own,
+    raw_n,
+    raw_w,
+    maps_n,
+    att_n,
+    att_w,
     row_max,
     row_sum,
     acc_n,
     acc_w,
+    lam,
     load_sem,
+    query_sem,
+    query_recv,
     recv_sem,
+    swap_sem,
+    whole_sem,
     up_sem,
-    first_sem,
-    second_sem,
-    pair_send,
-    pair_recv,
-    pair_ready,
+    peer_sem,
+    pair_sem,
+    relay_sem,
+    out_send,
+    out_recv,
+    lam_sem,
 ):
-    planes, rows, columns, tp_count = dims
+    planes, rows, columns, _tp_count = dims
     per_plane = rows * columns
+    pairs = columns // 2
+    grid = rows * pairs
     sp = lax.axis_index("sp")
     tp = lax.axis_index("tp")
     plane = sp // per_plane
     cell = sp % per_plane
     y = cell // columns
     x = cell % columns
-    queries = qn_ref.shape[2]
+    side = x % 2
+    across = cell + 1 - 2 * side
+    across_sp = plane * per_plane + across
+    query_cell = cell - side + tp
+    queries = qn_ref.shape[0]
     half_rows = queries // 2
-
-    own = []
-    begin = 0
-    for index, ref in enumerate((kn_ref, vn_ref, kw_ref, vw_ref)):
-        width = ref.shape[1]
-        own.append(
-            pltpu.make_async_copy(ref, kv.at[0, cell, :, pl.ds(begin, width)], load_sem.at[index])
-        )
-        begin += width
-    for copy in own:
-        copy.start()
-
-    def line(axis):
-        if axis == 0:
-            return [((y + k) % rows) * columns + x for k in range(1, rows)]
-        return [y * columns + (x + k) % columns for k in range(1, columns)]
-
-    def crossed(other, axis):
-        oy = other // columns
-        ox = other % columns
-        if axis == 0:
-            return [((oy + k) % rows) * columns + ox for k in range(1, rows)]
-        return [oy * columns + (ox + k) % columns for k in range(1, columns)]
+    at_home = side == tp
+    away = side != tp
+
+    def loads(into):
+        copies = []
+        begin = 0
+        for index, ref in enumerate((kn_ref, vn_ref, kw_ref, vw_ref)):
+            width = ref.shape[1]
+            copies.append(
+                pltpu.make_async_copy(ref, into.at[:, pl.ds(begin, width)], load_sem.at[index])
+            )
+            begin += width
+        return copies
+
+    def query_loads():
+        return [
+            pltpu.make_async_copy(qn_ref, raw_n, query_sem.at[0]),
+            pltpu.make_async_copy(qw_ref, raw_w, query_sem.at[1]),
+        ]
+
+    def query_swaps():
+        return [
+            pltpu.make_async_remote_copy(
+                src_ref=source,
+                dst_ref=target,
+                send_sem=query_sem.at[index],
+                recv_sem=query_recv.at[index],
+                device_id={"sp": across_sp, "tp": 1 - tp},
+                device_id_type=MESH,
+            )
+            for index, (source, target) in enumerate(((qn_ref, raw_n), (qw_ref, raw_w)))
+        ]
+
+    @pl.when(at_home)
+    def _():
+        for copy in loads(kv.at[0, cell]) + query_loads():
+            copy.start()
+
+    @pl.when(away)
+    def _():
+        for copy in loads(own):
+            copy.start()
+
+    def peer(k):
+        place = (y * pairs + x // 2 + k) % grid
+        return place // pairs * columns + place % pairs * 2 + side
 
     barrier = pltpu.get_barrier_semaphore()
-    for other in line(0) + line(1):
-        pl.semaphore_signal(
-            barrier, inc=1, device_id={"sp": plane * per_plane + other}, device_id_type=MESH
-        )
-    for k in range(1, tp_count):
-        pl.semaphore_signal(
-            barrier, inc=1, device_id={"tp": (tp + k) % tp_count}, device_id_type=MESH
-        )
+
+    def greet(device):
+        pl.semaphore_signal(barrier, inc=1, device_id=device, device_id_type=MESH)
+
+    for k in range(1, grid):
+        greet({"sp": plane * per_plane + peer(k)})
+    greet({"tp": 1 - tp})
+    for core in range(2):
+        greet({"sp": across_sp, "tp": core})
 
     @pl.when(plane > 0)
     def _():
-        pl.semaphore_signal(barrier, inc=1, device_id={"sp": sp - per_plane}, device_id_type=MESH)
+        greet({"sp": sp - per_plane})
 
     @pl.when(plane < planes - 1)
     def _():
-        pl.semaphore_signal(barrier, inc=1, device_id={"sp": sp + per_plane}, device_id_type=MESH)
+        greet({"sp": sp + per_plane})
 
     below = (plane > 0).astype(jnp.int32)
     above = (plane < planes - 1).astype(jnp.int32)
-    pl.semaphore_wait(barrier, rows - 1 + columns - 1 + tp_count - 1 + below + above)
-
-    for copy in own:
-        copy.wait()
+    pl.semaphore_wait(barrier, grid - 1 + 3 + below + above)
 
     def piece(depth, block, half):
-        return kv.at[depth, block, pl.ds(half * half_rows, half_rows), :]
-
-    def remote(depth, to_depth, block, half, target, send):
+        return kv.at[depth, block, pl.ds(pl.multiple_of(half * half_rows, half_rows), half_rows), :]
+
+    def remote(source, depth, block, half, device, send):
         return pltpu.make_async_remote_copy(
-            src_ref=piece(depth, block, half),
-            dst_ref=piece(to_depth, block, half),
+            src_ref=source,
+            dst_ref=piece(depth, block, half),
             send_sem=send,
-            recv_sem=recv_sem.at[to_depth, block, half],
-            device_id={"sp": target},
+            recv_sem=recv_sem.at[depth, block, half],
+            device_id=device,
             device_id_type=MESH,
         )
 
     def arrived(depth, block, half):
-        pltpu.make_async_remote_copy(
-            src_ref=piece(depth, block, half),
-            dst_ref=piece(depth, block, half),
-            send_sem=up_sem.at[0, 0],
-            recv_sem=recv_sem.at[depth, block, half],
-            device_id={"sp": sp},
-            device_id_type=MESH,
+        remote(
+            piece(depth, block, half), depth, block, half, {"sp": sp}, up_sem.at[0, 0]
         ).wait_recv()
 
-    def up_copies(depth):
+    def swap_copies():
         return [
-            remote(depth, depth + 1, cell, half, sp + per_plane, up_sem.at[depth, half])
+            remote(
+                own.at[pl.ds(core * half_rows, half_rows), :],
+                0,
+                cell,
+                core,
+                {"sp": across_sp, "tp": core},
+                swap_sem.at[core],
+            )
+            for core in range(2)
+        ]
+
+    def whole_copies():
+        return [
+            remote(piece(0, cell, half), 0, cell, half, {"tp": 1 - tp}, whole_sem.at[half])
             for half in range(2)
         ]
 
-    def direct_copies(depth):
-        copies = []
-        for half in range(2):
-            for k, other in enumerate(line(half)):
-                copies.append(
-                    remote(
-                        depth,
-                        depth,
-                        cell,
-                        half,
-                        plane * per_plane + other,
-                        first_sem.at[depth, half, k],
-                    )
-                )
-            for k, other in enumerate(line(1 - half)):
-                copies.append(
-                    remote(
-                        depth,
-                        depth,
-                        cell,
-                        half,
-                        plane * per_plane + other,
-                        second_sem.at[depth, half, 0, k],
-                    )
-                )
-        return copies
-
-    def relay_copies(depth):
-        groups = []
-        for half in range(2):
-            for i, block in enumerate(line(half)):
-                copies = [
-                    remote(
-                        depth,
-                        depth,
-                        block,
-                        half,
-                        plane * per_plane + other,
-                        second_sem.at[depth, half, i + 1, k],
-                    )
-                    for k, other in enumerate(line(1 - half))
-                ]
-                groups.append((block, half, copies))
-        return groups
-
-    def issue(depth):
+    def up_copy(depth, which):
+        block = cell if which == 0 else across
+        return remote(
+            piece(depth, block, tp),
+            depth + 1,
+            block,
+            tp,
+            {"sp": sp + per_plane},
+            up_sem.at[depth, which],
+        )
+
+    def peer_copies(depth, which):
+        block = cell if which == 0 else across
+        return [
+            remote(
+                piece(depth, block, tp),
+                depth,
+                block,
+                tp,
+                {"sp": plane * per_plane + peer(k)},
+                peer_sem.at[depth, which, k],
+            )
+            for k in range(1, grid)
+        ]
+
+    def pair_copy(depth, which):
+        block = cell if which == 0 else across
+        return remote(
+            piece(depth, block, tp), depth, block, tp, {"tp": 1 - tp}, pair_sem.at[depth, which]
+        )
+
+    def relay_copy(depth, which, k):
+        block = peer(k)
+        if which == 1:
+            block = block + 1 - 2 * side
+        return remote(
+            piece(depth, block, tp), depth, block, tp, {"tp": 1 - tp}, relay_sem.at[depth, which, k]
+        )
+
+    def spread(depth, which):
         @pl.when(plane < planes - 1)
         def _():
-            for copy in up_copies(depth):
-                copy.start()
-
-        for copy in direct_copies(depth):
+            up_copy(depth, which).start()
+
+        for copy in peer_copies(depth, which):
             copy.start()
 
+    def line(depth):
+        for which, block in enumerate((cell, across)):
+            arrived(depth, block, tp)
+            spread(depth, which)
+            pair_copy(depth, which).start()
+
     def relay(depth):
-        for block, half, copies in relay_copies(depth):
-            arrived(depth, block, half)
-            for copy in copies:
-                copy.start()
+        for which in range(2):
+            for k in range(1, grid):
+                block = peer(k) if which == 0 else peer(k) + 1 - 2 * side
+                arrived(depth, block, tp)
+                relay_copy(depth, which, k).start()
 
     def finish(depth):
-        for half in range(2):
-            for block in line(1 - half):
-                arrived(depth, block, half)
-            for first in line(half):
-                for block in crossed(first, 1 - half):
-                    arrived(depth, block, half)
-
+        for k in range(1, grid):
+            arrived(depth, peer(k), 1 - tp)
+            arrived(depth, peer(k) + 1 - 2 * side, 1 - tp)
+
+    lam_copy = pltpu.make_async_remote_copy(
+        src_ref=lam_ref,
+        dst_ref=lam,
+        send_sem=lam_sem.at[0],
+        recv_sem=lam_sem.at[1],
+        device_id={"tp": 1 - tp},
+        device_id_type=MESH,
+    )
+
+    @pl.when(at_home)
+    def _():
+        for copy in loads(kv.at[0, cell]):
+            copy.wait()
+        for copy in whole_copies():
+            copy.start()
+        lam_copy.start()
+        lam[...] = lam_ref[...]
+
+    @pl.when(away)
+    def _():
+        for copy in loads(own):
+            copy.wait()
+        for copy in swap_copies() + query_swaps():
+            copy.start()
+        arrived(0, cell, tp)
+
+    spread(0, 0)
     row_max[...] = jnp.full_like(row_max, MASKED)
     row_sum[...] = jnp.zeros_like(row_sum)
     acc_n[...] = jnp.zeros_like(acc_n)
     acc_w[...] = jnp.zeros_like(acc_w)
-    heads_n = qn_ref.shape[0]
+    heads_n = maps_n.shape[0]
+    width_k = kn_ref.shape[1]
     heads_w = qw_ref.shape[1] // kw_ref.shape[1]
-    width_k = kn_ref.shape[1]
     value_n = vn_ref.shape[1]
     begin_kw = width_k + value_n
     map_w = kw_ref.shape[1] // 2
@@ -262,7 +332,7 @@
 
             mask = None
             if masked:
-                query_pos = cell * queries + lax.broadcasted_iota(
+                query_pos = query_cell * queries + lax.broadcasted_iota(
                     jnp.int32, (queries, key_rows), 0
                 )
                 key_pos = at * queries + lax.broadcasted_iota(jnp.int32, (queries, key_rows), 1)
@@ -274,7 +344,7 @@
                 for which in range(2):
                     index = head * 2 + which
                     tile(
-                        qn_ref[head, which],
+                        maps_n[head, which],
                         key,
                         value,
                         DN**-0.5 * LOG2E,
@@ -290,7 +360,7 @@
                 for which in range(2):
                     index = head * 2 + which
                     tile(
-                        qw_ref[:, pl.ds(pl.multiple_of(index * map_w, map_w), map_w)],
+                        raw_w[:, pl.ds(pl.multiple_of(index * map_w, map_w), map_w)],
                         columns_of(begin_kw + which * map_w, map_w),
                         value,
                         DW**-0.5 * LOG2E,
@@ -314,91 +384,171 @@
 
             lax.fori_loop(0, per_plane // chunk, step, 0)
 
-    def advance(depth):
+    arrived(0, across, tp)
+    spread(0, 1)
+    pair_copy(0, 1).start()
+    relay(0)
+
+    @pl.when(plane > 0)
+    def _():
+        line(1)
+
+    @pl.when(at_home)
+    def _():
+        for copy in query_loads():
+            copy.wait()
+
+    @pl.when(away)
+    def _():
+        for copy in query_swaps():
+            copy.wait()
+
+    for head in range(heads_n):
+        both = raw_n[:, head * width_k : (head + 1) * width_k]
+        lane = lax.broadcasted_iota(jnp.int32, both.shape, 1)
+        zero = jnp.zeros_like(both)
+        maps_n[head, 0] = jnp.where(lane < DN, both, zero)
+        maps_n[head, 1] = jnp.where(lane < DN, zero, both)
+
+    @pl.when(away)
+    def _():
+        arrived(0, cell, 1 - tp)
+        lam_copy.wait_recv()
+
+    arrived(0, across, 1 - tp)
+    finish(0)
+    attend(0, True)
+
+    def depth_step(depth, carry):
+        relay(depth)
+
         @pl.when(depth < plane)
         def _():
-            for half in range(2):
-                arrived(depth + 1, cell, half)
-            issue(depth + 1)
-
-    def relay_next(depth):
-        @pl.when(depth < plane)
-        def _():
-            relay(depth + 1)
-
-    issue(0)
-    relay(0)
-    advance(0)
-    finish(0)
-    attend(0, True)
-    relay_next(0)
-
-    def depth_step(depth, carry):
-        advance(depth)
+            line(depth + 1)
+
+        arrived(depth, cell, 1 - tp)
+        arrived(depth, across, 1 - tp)
         finish(depth)
         attend(depth, False)
-        relay_next(depth)
         return carry
 
     lax.fori_loop(1, plane + 1, depth_step, 0)
 
-    def close(first, second, lam, gain):
-        head = first - lam * second
+    def close(first, second, weight, gain):
+        head = first - weight * second
         scale = lax.rsqrt(jnp.mean(head * head, axis=1, keepdims=True) + EPS)
         return (head * scale * gain).astype(jnp.bfloat16)
 
     for head in range(heads_n):
         maps = [acc_n[2 * head + k] / row_sum[2 * head + k][:, :1] for k in range(2)]
-        att[:, head * value_n : (head + 1) * value_n] = close(
-            maps[0], maps[1], lamn_ref[head], gainn_ref[...]
-        )
-    begin_w = heads_n * value_n
+        att_n[:, head * value_n : (head + 1) * value_n] = close(
+            maps[0], maps[1], lam[head : head + 1, :1], gainn_ref[...]
+        )
+    share = outn_ref.shape[0]
+    home_sp = plane * per_plane + query_cell
+
+    def out_copies(kind, core):
+        att, out = ((att_n, outn_ref), (att_w, outw_ref))[kind]
+        width = att.shape[1]
+        return pltpu.make_async_remote_copy(
+            src_ref=att.at[pl.ds(pl.multiple_of(core * share, share), share), :],
+            dst_ref=out.at[:, pl.ds(pl.multiple_of(side * width, width), width)],
+            send_sem=out_send.at[kind, core],
+            recv_sem=out_recv.at[kind, side],
+            device_id={"sp": home_sp, "tp": core},
+            device_id_type=MESH,
+        )
+
+    def send_out(kind, act):
+        @pl.when(at_home)
+        def _():
+            act(out_copies(kind, 1 - tp))
+
+        @pl.when(away)
+        def _():
+            for core in range(2):
+                act(out_copies(kind, core))
+
+    def keep(kind):
+        att, out = ((att_n, outn_ref), (att_w, outw_ref))[kind]
+        width = att.shape[1]
+
+        @pl.when(at_home)
+        def _():
+            out[:, pl.ds(pl.multiple_of(side * width, width), width)] = att[
+                pl.ds(pl.multiple_of(tp * share, share), share), :
+            ]
+
+    def start(copy):
+        copy.start()
+
+    def wait_send(copy):
+        copy.wait_send()
+
+    def out_arrived(kind, group):
+        att, out = ((att_n, outn_ref), (att_w, outw_ref))[kind]
+        width = att.shape[1]
+        block = out.at[:, pl.ds(pl.multiple_of(group * width, width), width)]
+        pltpu.make_async_remote_copy(
+            src_ref=block,
+            dst_ref=block,
+            send_sem=out_send.at[kind, 0],
+            recv_sem=out_recv.at[kind, group],
+            device_id={"sp": sp},
+            device_id_type=MESH,
+        ).wait_recv()
+
+    send_out(0, start)
     for head in range(heads_w):
         maps = [
             acc_w[2 * head + k] / row_sum[2 * (heads_n + head) + k][:, :1] for k in range(2)
         ]
-        att[:, begin_w + head * value_w : begin_w + (head + 1) * value_w] = close(
-            maps[0], maps[1], lamw_ref[head], gainw_ref[...]
-        )
-
-    def drain(depth, carry):
+        att_w[:, head * value_w : (head + 1) * value_w] = close(
+            maps[0], maps[1], lam[heads_n + head : heads_n + head + 1, :1], gainw_ref[...]
+        )
+    send_out(1, start)
+    keep(0)
+    keep(1)
+
+    @pl.when(at_home)
+    def _():
+        for copy in whole_copies():
+            copy.wait_send()
+        lam_copy.wait_send()
+
+    @pl.when(away)
+    def _():
+        for copy in swap_copies():
+            copy.wait_send()
+
+    def drain_line(depth, which):
         @pl.when(plane < planes - 1)
         def _():
-            for copy in up_copies(depth):
-                copy.wait_send()
-
-        for copy in direct_copies(depth):
+            up_copy(depth, which).wait_send()
+
+        for copy in peer_copies(depth, which):
             copy.wait_send()
-        for _block, _half, copies in relay_copies(depth):
-            for copy in copies:
-                copy.wait_send()
+        for k in range(1, grid):
+            relay_copy(depth, which, k).wait_send()
+
+    def drain(depth, carry):
+        for which in range(2):
+            drain_line(depth, which)
+            pair_copy(depth, which).wait_send()
         return carry
 
-    lax.fori_loop(0, plane + 1, drain, 0)
-    for k in range(1, tp_count):
-        pl.semaphore_signal(
-            pair_ready, inc=1, device_id={"tp": (tp + k) % tp_count}, device_id_type=MESH
-        )
-    pl.semaphore_wait(pair_ready, tp_count - 1)
-    share = out_ref.shape[1]
-    copies = []
-    for k in range(1, tp_count):
-        other = (tp + k) % tp_count
-        copies.append(
-            pltpu.make_async_remote_copy(
-                src_ref=att.at[pl.ds(pl.multiple_of(other * share, share), share), :],
-                dst_ref=out_ref.at[tp],
-                send_sem=pair_send.at[k - 1],
-                recv_sem=pair_recv.at[k - 1],
-                device_id={"tp": other},
-                device_id_type=MESH,
-            )
-        )
-    for copy in copies:
-        copy.start()
-    out_ref[tp] = att[pl.ds(pl.multiple_of(tp * share, share), share), :]
-    for copy in copies:
-        copy.wait()
+    drain_line(0, 0)
+    drain_line(0, 1)
+    pair_copy(0, 1).wait_send()
+    lax.fori_loop(1, plane + 1, drain, 0)
+    for kind in range(2):
+        out_arrived(kind, 1 - side)
+
+        @pl.when(away)
+        def _(kind=kind):
+            out_arrived(kind, side)
+
+        send_out(kind, wait_send)
 
 
 def attended_rows(
@@ -419,58 +569,66 @@
     count = queries_narrow.shape[0]
     heads_n = queries_narrow.shape[1] // (2 * DN)
     heads_w = queries_wide.shape[1] // (2 * DW)
-    maps = queries_narrow.reshape(count, heads_n, 2, DN).transpose(1, 2, 0, 3)
-    padded = jnp.stack(
-        [
-            jnp.pad(maps[:, 0], ((0, 0), (0, 0), (0, DN))),
-            jnp.pad(maps[:, 1], ((0, 0), (0, 0), (DN, 0))),
-        ],
-        axis=1,
-    )
     width = (
         keys_narrow.shape[1] + values_narrow.shape[1] + keys_wide.shape[1] + values_wide.shape[1]
     )
     per_plane = rows * columns
-    features = heads_n * VN + heads_w * VW
-    longest = max(rows, columns)
+    grid = per_plane // 2
     tiles = 2 * (heads_n + heads_w)
+    share = count // tp_count
     vmem = pl.BlockSpec(memory_space=pltpu.VMEM)
-    smem = pl.BlockSpec(memory_space=pltpu.SMEM)
+    lambdas = jnp.concatenate([lambda_narrow, lambda_wide])
+    lambdas = jnp.pad(lambdas, (0, -lambdas.shape[0] % 8))
+    lambdas = jnp.broadcast_to(lambdas[:, None], (lambdas.shape[0], 128))
     hbm = pl.BlockSpec(memory_space=pl.ANY)
+    dma = pltpu.SemaphoreType.DMA
     return pl.pallas_call(
         functools.partial(attend_kernel, (planes, rows, columns, tp_count)),
-        out_shape=jax.ShapeDtypeStruct((tp_count, count // tp_count, features), jnp.bfloat16),
-        in_specs=[vmem, hbm, hbm, vmem, hbm, hbm, smem, smem, vmem, vmem],
-        out_specs=vmem,
+        out_shape=[
+            jax.ShapeDtypeStruct((share, tp_count * heads_n * VN), jnp.bfloat16),
+            jax.ShapeDtypeStruct((share, tp_count * heads_w * VW), jnp.bfloat16),
+        ],
+        in_specs=[hbm, hbm, hbm, hbm, hbm, hbm, vmem, vmem, vmem],
+        out_specs=[vmem, vmem],
         scratch_shapes=[
             pltpu.VMEM((planes, per_plane, count, width), jnp.bfloat16),
-            pltpu.VMEM((count, features), jnp.bfloat16),
+            pltpu.VMEM((count, width), jnp.bfloat16),
+            pltpu.VMEM(queries_narrow.shape, jnp.bfloat16),
+            pltpu.VMEM(queries_wide.shape, jnp.bfloat16),
+            pltpu.VMEM((heads_n, 2, count, 2 * DN), jnp.bfloat16),
+            pltpu.VMEM((count, heads_n * VN), jnp.bfloat16),
+            pltpu.VMEM((count, heads_w * VW), jnp.bfloat16),
             pltpu.VMEM((tiles, count, 128), jnp.float32),
             pltpu.VMEM((tiles, count, 128), jnp.float32),
             pltpu.VMEM((2 * heads_n, count, VN), jnp.float32),
             pltpu.VMEM((2 * heads_w, count, VW), jnp.float32),
-            pltpu.SemaphoreType.DMA((4,)),
-            pltpu.SemaphoreType.DMA((planes, per_plane, 2)),
-            pltpu.SemaphoreType.DMA((planes, 2)),
-            pltpu.SemaphoreType.DMA((planes, 2, longest)),
-            pltpu.SemaphoreType.DMA((planes, 2, longest, longest)),
-            pltpu.SemaphoreType.DMA((max(1, tp_count - 1),)),
-            pltpu.SemaphoreType.DMA((max(1, tp_count - 1),)),
-            pltpu.SemaphoreType.REGULAR,
+            pltpu.VMEM(lambdas.shape, jnp.float32),
+            dma((4,)),
+            dma((2,)),
+            dma((2,)),
+            dma((planes, per_plane, 2)),
+            dma((2,)),
+            dma((2,)),
+            dma((planes, 2)),
+            dma((planes, 2, grid)),
+            dma((planes, 2)),
+            dma((planes, 2, grid)),
+            dma((2, 2)),
+            dma((2, 2)),
+            dma((2,)),
         ],
         compiler_params=pltpu.CompilerParams(
             collective_id=0, has_side_effects=True, vmem_limit_bytes=56 * 1024 * 1024
         ),
         name="gather_attend",
     )(
-        padded,
+        queries_narrow,
         keys_narrow,
         values_narrow,
         queries_wide,
         keys_wide,
         values_wide,
-        lambda_narrow,
-        lambda_wide,
+        lambdas,
         gain_narrow.reshape(1, -1),
         gain_wide.reshape(1, -1),
     )
@@ -972,7 +1130,7 @@
     route_weights,
 ):
     sp_count = lax.axis_size("sp")
-    attended = attended_rows(
+    narrow_rows, wide_rows = attended_rows(
         sp_count,
         lax.axis_size("tp"),
         queries_narrow,
@@ -986,10 +1144,6 @@
         gain_narrow,
         gain_wide,
     )
-    narrow_width = out_narrow.shape[0] // attended.shape[0]
-    attended = attended.transpose(1, 0, 2)
-    narrow_rows = attended[:, :, :narrow_width].reshape(attended.shape[0], -1)
-    wide_rows = attended[:, :, narrow_width:].reshape(attended.shape[0], -1)
     projected = jnp.dot(narrow_rows, out_narrow, preferred_element_type=jnp.float32) + jnp.dot(
         wide_rows, out_wide, preferred_element_type=jnp.float32
     )

time: 227 us -> 211 us (0.930)
  Pallas kernels: 190 us -> 180 us
  local copies, waits for them, and re-layouts: 9.16 us -> 5.83 us
    pallas_call x1, Pallas kernels: 104 us -> 94.3 us  [dispatched_rows(): pl.pallas_call(functools.partial(dispatch_kernel, dims, group), out_shape...]
    slice x4 -> x1, local copies, waits for them, and re-layouts: 2.97 us -> 0.22 us  [the longest x2 1.91 us: shards(): wide_rows = attended[:, :, narrow_width:].reshape(attended.shape[0], -1)]
where the time goes in v2:
time: 211 us; the launch traced here: 210 us
  Pallas kernels  180 us (85%)
  matrix products  17.7 us (8%)
  other arithmetic  7.04 us (3%)
  local copies, waits for them, and re-layouts  5.83 us (3%)
    pallas_call x1, Pallas kernels, dispatched_rows(): pl.pallas_call(functools.partial(dispatch_kernel, dims, group), out_shape...  94.3 us
    pallas_call x1, Pallas kernels, combined_rows(): pl.pallas_call(functools.partial(combine_kernel, dims, group, chunks), ou...  51 us
    pallas_call x1, Pallas kernels, attended_rows(): pl.pallas_call(functools.partial(attend_kernel, (planes, rows, columns, t...  34.3 us
    dot_general x1, matrix products, run_experts(): jnp.einsum('rjcd,jdf->rjcf', grouped, expert_gate, preferred_element_type...  4.74 us
    dot_general x1, matrix products, shards(): jnp.dot(shared_hidden, shared_down, preferred_element_type=jnp.float32)  4.35 us

profile of v2, /device:TPU:0, one launch (start us, length us, event | category | flops | bytes accessed | tf_op | source)
XLA Modules:
  0.0 210.3 jit_solution(2559598854383324844)
XLA Ops:
  0.0 0.9 fusion.35
  0.9 0.7 broadcast_in_dim.2.lam_ref
  1.6 34.3 %gather_attend.1 = (bf16[128,1024]{1,0:T(8,128)(2,1)}, bf16[128,1024]{1,0:T(8,128)(2,1)}) custom-call(bf16[256,512]{1,0:T(8,128)(2,1)} %qn_ref.1, bf16[256,128]{1,0:T(8,128)(2,1)} %kn_ref.1, bf16[256,128]{1,0:T(8,128)(2,1)} %vn_ref.1, bf16[256,512]{1,0:T(8,128)(2,1)} %qw_ref.1, bf16[256,256]{1,0:T(8,128)(2,1)} %kw_ref.1, bf16[256,256]{1,0:T(8,128)(2,1)} %vw_ref.1, ...), custom_call_target="tpu_custom_call" | custom-call | tf_op jit(solution)/shard_map/gather_attend/pallas_call | solution.py:585
  35.8 3.1 %fusion.37 = f32[128,2048]{1,0:T(8,128)S(1)} fusion(bf16[128,1024]{1,0:T(8,128)(2,1)} %get-tuple-element.9, bf16[1024,2048]{1,0:T(8,128)(2,1)} %param.34), kind=kOutput, calls=%fused_computation.62 | convolution fusion | flops 536870912 | bytes 5505024 | tf_op jit(solution)/shard_map/dot_general | solution.py:1147
  39.0 0.4 copy-done.2
  39.4 0.0 copy-done.6
  39.4 0.9 multiply_reduce_fusion.1
  40.3 0.1 copy-done.5
  40.4 0.4 fusion.17
  40.8 0.2 copy-done.8
  41.0 1.0 fusion.19.normed_ref
  42.0 0.1 copy.28
  42.1 0.1 eq.29
  42.2 1.2 reduce-window.6
  43.4 0.2 slice_reduce_fusion
  43.7 0.1 eq.25
  43.8 0.1 fusion.33
  43.9 0.1 reduce_sum.41
  44.0 0.1 copy.31
  44.1 0.6 maximum_bitcast_fusion.slots_ref
  44.7 94.3 %dispatch.1 = (bf16[2,16,48,2048]{3,2,1,0:T(8,128)(2,1)}, f32[4,8,128]{2,1,0:T(8,128)}) custom-call(bf16[128,2048]{1,0:T(8,128)(2,1)} %fusion.19.normed_ref, f32[8,128]{1,0:T(8,128)} %maximum_bitcast_fusion.slots_ref), custom_call_target="tpu_custom_call" | custom-call | tf_op jit(solution)/shard_map/dispatch/pallas_call | solution.py:839
  139.0 4.7 %fusion.2 = f32[2,32,24,256]{3,2,1,0:T(8,128)S(1)} fusion(bf16[32,2,24,2048]{3,2,1,0:T(8,128)(2,1)} %bitcast.84, bf16[2,2048,256]{2,1,0:T(8,128)(2,1)S(1)} %copy-done), kind=kOutput, calls=%fused_computation.3 | convolution fusion | flops 1610612736 | bytes 9961472 | tf_op jit(solution)/shard_map/rjcd,jdf->rjcf/dot_general | solution.py:1089
  143.8 0.4 copy-done.13
  144.2 2.2 %fusion.8 = bf16[32,2,24,256]{3,2,0,1:T(8,128)(2,1)S(1)} fusion(f32[2,32,24,256]{3,2,1,0:T(8,128)S(1)} %fusion.2, bf16[2,2048,256]{2,1,0:T(8,128)(2,1)S(1)} %copy-done.13, bf16[32,2,24,2048]{3,2,1,0:T(8,128)(2,1)S(1)} %bitcast.85), kind=kOutput, calls=%fused_computation.14 | convolution fusion | flops 1612972032 | bytes 10747904 | tf_op jit(solution)/shard_map/rjcd,jdf->rjcf/dot_general | solution.py:1092
  146.4 1.0 fusion.4
  147.4 1.0 fusion.5
  148.4 0.6 pad_maximum_fusion
  149.0 3.2 %copy.34 = bf16[32,2,24,2048]{3,2,1,0:T(8,128)(2,1)} copy(bf16[32,2,24,2048]{3,2,0,1:T(8,128)(2,1)S(1)} %pad_maximum_fusion) | data formatting | bytes 12582912 | tf_op jit(solution)/shard_map/stack | solution.py:1094
  152.2 51.0 %combine.1 = f32[128,2048]{1,0:T(8,128)} custom-call(bf16[2,16,48,2048]{3,2,1,0:T(8,128)(2,1)} %bitcast.81, f32[4,8,128]{2,1,0:T(8,128)} %get-tuple-element.12.marks_ref), custom_call_target="tpu_custom_call" | custom-call | tf_op jit(solution)/shard_map/combine/pallas_call | solution.py:1058
  203.2 0.4 fusion.38
  203.7 4.4 %multiply_reduce_fusion = (f32[128]{0:T(128)S(1)}, f32[128,2048]{1,0:T(8,128)}) fusion(f32[128,2048]{1,0:T(8,128)} %combine.1, bf16[512,2048]{1,0:T(8,128)(2,1)} %param.42, bf16[128,2048]{1,0:T(8,128)(2,1)S(1)} %copy-done.1, bf16[2048,512]{1,0:T(8,128)(2,1)} %param.41, f32[128,512]{1,0:T(8,128)S(1)} %fusion.38), kind=kOutput, calls=%fused_computation.31 | convolution fusion | flops 538050432 | bytes 7078400 | tf_op jit(solution)/shard_map/dot_general | solution.py:1183
  208.1 2.2 %fusion.20 = bf16[128,2048]{1,0:T(8,128)(2,1)} fusion(bf16[128,2048]{1,0:T(8,128)(2,1)S(1)} %get-tuple-element.14, f32[128,2048]{1,0:T(8,128)} %get-tuple-element.18, f32[2048]{0:T(1024)S(1)} %copy-done.9, f32[128]{0:T(128)S(1)} %add_rsqrt_fusion), kind=kLoop, calls=%fused_computation.28 | loop fusion | flops 1310720 | bytes 2105856 | tf_op jit(solution)/shard_map/convert_element_type | solution.py:1185
  (30 shorter events, 0.1 us)
Async XLA Ops:
  0.0 139.0 %copy-start = (bf16[2,2048,256]{2,1,0:T(8,128)(2,1)S(1)}, bf16[2,2048,256]{2,1,0:T(8,128)(2,1)}, u32[]{:S(2)}) copy-start(bf16[2,2048,256]{2,1,0:T(8,128)(2,1)} %param.43) | copy-start | bytes 6291460
  35.8 3.5 %copy-start.2 = (bf16[1024,2048]{1,0:T(8,128)(2,1)S(1)}, bf16[1024,2048]{1,0:T(8,128)(2,1)}, u32[]{:S(2)}) copy-start(bf16[1024,2048]{1,0:T(8,128)(2,1)} %param.35) | copy-start | bytes 12582916
  35.8 3.5 %copy-start.6 = (bf16[128,1024]{1,0:T(8,128)(2,1)S(1)}, bf16[128,1024]{1,0:T(8,128)(2,1)}, u32[]{:S(2)}) copy-start(bf16[128,1024]{1,0:T(8,128)(2,1)} %get-tuple-element.10) | copy-start | bytes 786436
  39.4 1.0 copy-start.5
  39.4 1.0 copy-start.7
  40.3 0.7 copy-start.8
  40.3 1.7 copy-start.10
  40.3 3.8 %copy-start.11 = (f32[128,4]{0,1:T(4,128)S(1)}, f32[128,4]{0,1:T(4,128)}, u32[]{:S(2)}) copy-start(f32[128,4]{0,1:T(4,128)} %param.47) | copy-start | bytes 6148
  139.0 4.8 %copy-start.12 = (bf16[2,16,48,2048]{3,2,1,0:T(8,128)(2,1)S(1)}, bf16[2,16,48,2048]{3,2,1,0:T(8,128)(2,1)}, u32[]{:S(2)}) copy-start(bf16[2,16,48,2048]{3,2,1,0:T(8,128)(2,1)} %get-tuple-element.11) | copy-start | bytes 18874372
  139.0 5.2 %copy-start.13 = (bf16[2,2048,256]{2,1,0:T(8,128)(2,1)S(1)}, bf16[2,2048,256]{2,1,0:T(8,128)(2,1)}, u32[]{:S(2)}) copy-start(bf16[2,2048,256]{2,1,0:T(8,128)(2,1)} %param.44) | copy-start | bytes 6291460
  144.2 2.2 %copy-start.4 = (bf16[2,256,2048]{2,1,0:T(8,128)(2,1)S(1)}, bf16[2,256,2048]{2,1,0:T(8,128)(2,1)}, u32[]{:S(2)}) copy-start(bf16[2,256,2048]{2,1,0:T(8,128)(2,1)} %param.45) | copy-start | bytes 6291460
  152.2 51.0 %copy-start.1 = (bf16[128,2048]{1,0:T(8,128)(2,1)S(1)}, bf16[128,2048]{1,0:T(8,128)(2,1)}, u32[]{:S(2)}) copy-start(bf16[128,2048]{1,0:T(8,128)(2,1)} %fusion.19.normed_ref) | copy-start | bytes 1572868
  152.2 51.0 %copy-start.3 = (bf16[2048,512]{1,0:T(8,128)(2,1)S(1)}, bf16[2048,512]{1,0:T(8,128)(2,1)}, u32[]{:S(2)}) copy-start(bf16[2048,512]{1,0:T(8,128)(2,1)} %param.40) | copy-start | bytes 6291460
  203.7 4.4 %copy-start.9 = (f32[2048]{0:T(1024)S(1)}, f32[2048]{0:T(1024)}, u32[]{:S(2)}) copy-start(f32[2048]{0:T(1024)} %param.39) | copy-start | bytes 24580

commit v3 on v2

--- a/solution.py
+++ b/solution.py
@@ -663,16 +663,37 @@
     return plane, cell, sp, tp
 
 
+def silu(values):
+    return values / (1.0 + jnp.exp(-values))
+
+
 def dispatch_kernel(
     dims,
     group,
+    chunks,
     normed_ref,
     slots_ref,
-    inbox,
+    gate_ref,
+    up_ref,
+    down_ref,
+    shared_gate_ref,
+    shared_up_ref,
+    shared_down_ref,
+    parts,
     marks,
+    shared_out,
     held,
     stage,
+    inbox,
+    result,
+    gate,
+    up,
+    down,
+    shared_gate,
+    shared_up,
+    shared_down,
     load_sem,
+    weight_sem,
     row_recv,
     mark_recv,
     row_send,
@@ -681,99 +702,121 @@
     cell_send,
     pair_recv,
     pair_send,
+    store_sem,
 ):
     planes, rows, columns, tp_count = dims
     per_plane = rows * columns
-    sp_now = lax.axis_index("sp")
-    mine = sp_now // per_plane
+    mine = lax.axis_index("sp") // per_plane
     loads = [
         pltpu.make_async_copy(normed_ref, held.at[mine], load_sem.at[0]),
         pltpu.make_async_copy(slots_ref, marks.at[mine], load_sem.at[1]),
     ]
-    for copy in loads:
+    weights = [
+        pltpu.make_async_copy(source, target, weight_sem.at[index])
+        for index, (source, target) in enumerate(
+            (
+                (shared_gate_ref, shared_gate),
+                (shared_up_ref, shared_up),
+                (shared_down_ref, shared_down),
+                (gate_ref, gate),
+                (up_ref, up),
+                (down_ref, down),
+            )
+        )
+    ]
+    for copy in loads + weights:
         copy.start()
     plane, cell, sp, tp = plane_greeting(planes, rows, columns, tp_count)
     for copy in loads:
         copy.wait()
     padded = stage.shape[2]
     token_count = held.shape[1]
-
-    def hops(source, way):
-        target = {"sp": (sp + per_plane * (1 if way == 0 else planes - 1)) % (planes * per_plane)}
-        return [
-            pltpu.make_async_remote_copy(
-                src_ref=marks.at[source],
-                dst_ref=marks.at[source],
-                send_sem=mark_send.at[source, way],
-                recv_sem=mark_recv.at[source],
-                device_id=target,
-                device_id_type=MESH,
-            ),
-            pltpu.make_async_remote_copy(
-                src_ref=held.at[source],
-                dst_ref=held.at[source],
-                send_sem=row_send.at[source, way],
-                recv_sem=row_recv.at[source],
-                device_id=target,
-                device_id_type=MESH,
-            ),
-        ]
-
-    def to_cell(source, k):
-        other = (cell + k) % per_plane
+    width = held.shape[2]
+    wide = width // chunks
+    local_experts = gate.shape[0]
+    capacity = group // local_experts
+
+    def span(chunk):
+        return pl.ds(chunk * wide, wide)
+
+    def mark_hop(source, way, target):
         return pltpu.make_async_remote_copy(
-            src_ref=stage.at[source, other],
-            dst_ref=inbox.at[tp, source * per_plane + cell],
-            send_sem=cell_send.at[source, k],
-            recv_sem=cell_recv.at[source, (per_plane - k) % per_plane],
-            device_id={"sp": plane * per_plane + other},
+            src_ref=marks.at[source],
+            dst_ref=marks.at[source],
+            send_sem=mark_send.at[source, way],
+            recv_sem=mark_recv.at[source],
+            device_id={"sp": target},
             device_id_type=MESH,
         )
 
-    def to_pair(source, k):
-        block = inbox.at[tp, pl.ds(source * per_plane, per_plane)]
+    def row_hop(source, chunk, way, target):
+        block = held.at[source, :, span(chunk)]
         return pltpu.make_async_remote_copy(
             src_ref=block,
             dst_ref=block,
-            send_sem=pair_send.at[source, k - 1],
-            recv_sem=pair_recv.at[source, k - 1],
+            send_sem=row_send.at[source, chunk, way],
+            recv_sem=row_recv.at[source, chunk],
+            device_id={"sp": target},
+            device_id_type=MESH,
+        )
+
+    def to_cell(source, chunk, k):
+        other = (cell + k) % per_plane
+        return pltpu.make_async_remote_copy(
+            src_ref=stage.at[source, other, :, span(chunk)],
+            dst_ref=inbox.at[source, tp, cell, :, span(chunk)],
+            send_sem=cell_send.at[source, chunk, k],
+            recv_sem=cell_recv.at[source, chunk, (per_plane - k) % per_plane],
+            device_id={"sp": plane * per_plane + other},
+            device_id_type=MESH,
+        )
+
+    def from_cell(source, chunk, k):
+        return pltpu.make_async_remote_copy(
+            src_ref=stage.at[source, cell, :, span(chunk)],
+            dst_ref=inbox.at[source, tp, (cell + k) % per_plane, :, span(chunk)],
+            send_sem=cell_send.at[source, chunk, k],
+            recv_sem=cell_recv.at[source, chunk, k],
+            device_id={"sp": sp},
+            device_id_type=MESH,
+        )
+
+    def to_pair(source, chunk, k):
+        block = inbox.at[source, tp, :, :, span(chunk)]
+        return pltpu.make_async_remote_copy(
+            src_ref=block,
+            dst_ref=block,
+            send_sem=pair_send.at[source, chunk, k - 1],
+            recv_sem=pair_recv.at[source, chunk, k - 1],
             device_id={"tp": (tp + k) % tp_count},
             device_id_type=MESH,
         )
 
-    steps = [(0, 0)] + [(d, way) for d in range(1, planes) for way in range(2)]
-
-    def of_step(d, way):
-        source = plane - d if way == 0 else plane + d
-        exists = source >= 0 if way == 0 else source < planes
-        return source, exists
-
-    def onward(source, d, way, act):
-        for side in ((0, 1) if d == 0 else (way,)):
-
-            @pl.when(plane < planes - 1 if side == 0 else plane > 0)
-            def _(side=side):
-                for copy in hops(source, side):
-                    act(copy)
-
-    def start(copy):
-        copy.start()
-
-    def wait_send(copy):
-        copy.wait_send()
-
-    def body(d, way):
-        source, exists = of_step(d, way)
-
-        @pl.when(exists)
+    def store(source):
+        return pltpu.make_async_copy(result.at[source], parts.at[source], store_sem.at[source])
+
+    def onward(source, act):
+        @pl.when((source <= plane) & (plane < planes - 1))
         def _():
-            if d > 0:
-                for copy in hops(source, way):
-                    copy.wait_recv()
-            onward(source, d, way, start)
-            tokens = held[source]
-            slots = marks[source]
-            row = lax.broadcasted_iota(jnp.int32, (padded, token_count), 0)
+            act(0, sp + per_plane)
+
+        @pl.when((source >= plane) & (plane > 0))
+        def _():
+            act(1, sp - per_plane)
+
+    def body(source, first):
+        if not first:
+            mark_hop(source, 0, sp).wait_recv()
+        onward(source, lambda way, target: mark_hop(source, way, target).start())
+        slots = marks[source]
+        row = lax.broadcasted_iota(jnp.int32, (padded, token_count), 0)
+        for chunk in range(chunks):
+            if not first:
+                row_hop(source, chunk, 0, sp).wait_recv()
+            onward(
+                source, lambda way, target: row_hop(source, chunk, way, target).start()
+            )
+            tokens = held[source, :, span(chunk)]
             for k in list(range(1, per_plane)) + [0]:
                 other = (cell + k) % per_plane
                 base = (plane * per_plane + other) * group
@@ -787,47 +830,96 @@
                     preferred_element_type=jnp.float32,
                 ).astype(jnp.bfloat16)
                 if k == 0:
-                    inbox[tp, source * per_plane + cell] = chosen
+                    inbox[source, tp, cell, :, span(chunk)] = chosen
                 else:
-                    stage[source, other] = chosen
+                    stage[source, other, :, span(chunk)] = chosen
+                    to_cell(source, chunk, k).start()
+
+    def finish(source):
+        for chunk in range(chunks):
             for k in range(1, per_plane):
-                to_cell(source, k).start()
-
-    def finish(d, way):
-        source, exists = of_step(d, way)
-
-        @pl.when(exists)
-        def _():
+                from_cell(source, chunk, k).wait_recv()
+            for k in range(1, tp_count):
+                to_pair(source, chunk, k).start()
+
+    def experts(source):
+        for chunk in range(chunks):
+            for k in range(1, tp_count):
+                to_pair(source, chunk, k).wait_recv()
+        done = 0
+        for index in range(local_experts):
+            begin = index * capacity // 16 * 16
+            end = -(-((index + 1) * capacity) // 16) * 16
+            block = (tp_count, per_plane, end - begin, width)
+            tokens = inbox[source, :, :, begin:end, :].reshape(-1, width)
+            gated = jnp.dot(tokens, gate[index], preferred_element_type=jnp.float32)
+            hidden = silu(gated) * jnp.dot(
+                tokens, up[index], preferred_element_type=jnp.float32
+            )
+            out = (
+                jnp.dot(
+                    hidden.astype(jnp.bfloat16), down[index], preferred_element_type=jnp.float32
+                )
+                .astype(jnp.bfloat16)
+                .reshape(block)
+            )
+            both = max(0, done - begin)
+            if both > 0:
+                shape = (tp_count, per_plane, both, width)
+                row = lax.broadcasted_iota(jnp.int32, shape, 2) + begin
+                result[source, :, :, begin:done, :] = jnp.where(
+                    row < index * capacity, result[source, :, :, begin:done, :], out[:, :, :both]
+                )
+            if end > begin + both:
+                result[source, :, :, begin + both : end, :] = out[:, :, both:]
+            done = max(done, end)
+        store(source).start()
+
+    body(plane, True)
+    for copy in weights[:3]:
+        copy.wait()
+    normed = held[plane]
+    shared_hidden = silu(
+        jnp.dot(normed, shared_gate[...], preferred_element_type=jnp.float32)
+    ) * jnp.dot(normed, shared_up[...], preferred_element_type=jnp.float32)
+    shared_out[...] = jnp.dot(
+        shared_hidden.astype(jnp.bfloat16), shared_down[...], preferred_element_type=jnp.float32
+    )
+    for copy in weights[3:]:
+        copy.wait()
+
+    def step(_, carry):
+        low, high, before = carry
+        use_high = (low < 0) | ((high < planes) & (high - plane <= plane - low))
+        source = jnp.where(use_high, high, low)
+        body(source, False)
+        finish(before)
+        experts(before)
+        return jnp.where(use_high, low, low - 1), jnp.where(use_high, high + 1, high), source
+
+    last = lax.fori_loop(0, planes - 1, step, (plane - 1, plane + 1, plane))[2]
+    finish(last)
+    experts(last)
+
+    def drain(source, carry):
+        onward(source, lambda way, target: mark_hop(source, way, target).wait_send())
+        for chunk in range(chunks):
+            onward(
+                source, lambda way, target: row_hop(source, chunk, way, target).wait_send()
+            )
             for k in range(1, per_plane):
-                pltpu.make_async_remote_copy(
-                    src_ref=stage.at[source, cell],
-                    dst_ref=inbox.at[tp, source * per_plane + (cell + k) % per_plane],
-                    send_sem=cell_send.at[source, k],
-                    recv_sem=cell_recv.at[source, k],
-                    device_id={"sp": sp},
-                    device_id_type=MESH,
-                ).wait_recv()
+                to_cell(source, chunk, k).wait_send()
             for k in range(1, tp_count):
-                to_pair(source, k).start()
-
-    for index, step in enumerate(steps):
-        body(*step)
-        if index > 0:
-            finish(*steps[index - 1])
-    finish(*steps[-1])
-    for d, way in steps:
-        source, exists = of_step(d, way)
-
-        @pl.when(exists)
-        def _(source=source, d=d, way=way):
-            onward(source, d, way, wait_send)
-            for k in range(1, per_plane):
-                to_cell(source, k).wait_send()
-            for k in range(1, tp_count):
-                to_pair(source, k).wait()
-
-
-def dispatched_rows(dims, group, normed, slot_index, route_weights):
+                to_pair(source, chunk, k).wait_send()
+        store(source).wait()
+        return carry
+
+    lax.fori_loop(0, planes, drain, 0)
+
+
+def dispatched_rows(
+    dims, group, normed, slot_index, route_weights, routed_weights, shared_weights
+):
     planes, rows, columns, tp_count = dims
     per_plane = rows * columns
     token_count, width = normed.shape
@@ -835,33 +927,46 @@
     slots = slot_index.reshape(token_count, TOPK).astype(jnp.float32)
     slots = jnp.concatenate([slots, route_weights], axis=1).T
     hbm = pl.BlockSpec(memory_space=pl.ANY)
+    vmem = pl.BlockSpec(memory_space=pltpu.VMEM)
     dma = pltpu.SemaphoreType.DMA
+    chunks = math.gcd(width // 512, 2)
+    pairs = max(1, tp_count - 1)
+    weights = list(routed_weights) + list(shared_weights)
+    inbox = (planes, tp_count, per_plane, padded, width)
     return pl.pallas_call(
-        functools.partial(dispatch_kernel, dims, group),
+        functools.partial(dispatch_kernel, dims, group, chunks),
         out_shape=[
-            jax.ShapeDtypeStruct((tp_count, planes * per_plane, padded, width), jnp.bfloat16),
+            jax.ShapeDtypeStruct(inbox, jnp.bfloat16),
             jax.ShapeDtypeStruct((planes, 2 * TOPK, token_count), jnp.float32),
+            jax.ShapeDtypeStruct((token_count, width), jnp.float32),
         ],
-        in_specs=[hbm, hbm],
-        out_specs=[pl.BlockSpec(memory_space=pltpu.VMEM)] * 2,
+        in_specs=[hbm] * (2 + len(weights)),
+        out_specs=[hbm, vmem, vmem],
         scratch_shapes=[
             pltpu.VMEM((planes, token_count, width), jnp.bfloat16),
             pltpu.VMEM((planes, per_plane, padded, width), jnp.bfloat16),
+            pltpu.VMEM(inbox, jnp.bfloat16),
+            pltpu.VMEM(inbox, jnp.bfloat16),
+        ]
+        + [pltpu.VMEM(weight.shape, jnp.bfloat16) for weight in weights]
+        + [
             dma((2,)),
+            dma((len(weights),)),
+            dma((planes, chunks)),
             dma((planes,)),
+            dma((planes, chunks, 2)),
+            dma((planes, 2)),
+            dma((planes, chunks, per_plane)),
+            dma((planes, chunks, per_plane)),
+            dma((planes, chunks, pairs)),
+            dma((planes, chunks, pairs)),
             dma((planes,)),
-            dma((planes, 2)),
-            dma((planes, 2)),
-            dma((planes, per_plane)),
-            dma((planes, per_plane)),
-            dma((planes, max(1, tp_count - 1))),
-            dma((planes, max(1, tp_count - 1))),
         ],
         compiler_params=pltpu.CompilerParams(
-            collective_id=1, has_side_effects=True, vmem_limit_bytes=56 * 1024 * 1024
+            collective_id=1, has_side_effects=True, vmem_limit_bytes=60 * 1024 * 1024
         ),
         name="dispatch",
-    )(normed, slots)
+    )(normed, slots, *weights)
 
 
 def combine_kernel(
@@ -870,6 +975,10 @@
     chunks,
     parts_ref,
     marks_ref,
+    mixed_ref,
+    shared_ref,
+    gain_ref,
+    layer_ref,
     out_ref,
     mine,
     theirs,
@@ -907,7 +1016,7 @@
 
     def load(source, chunk):
         return pltpu.make_async_copy(
-            parts_ref.at[tp, pl.ds(source * per_plane, per_plane), :, span(chunk)],
+            parts_ref.at[source, tp, :, :, span(chunk)],
             mine.at[source, :, :, span(chunk)],
             load_sem.at[source, chunk],
         )
@@ -915,7 +1024,7 @@
     def to_pair(source, chunk, k):
         other = (tp + k) % tp_count
         return pltpu.make_async_remote_copy(
-            src_ref=parts_ref.at[other, pl.ds(source * per_plane, per_plane), :, span(chunk)],
+            src_ref=parts_ref.at[source, other, :, :, span(chunk)],
             dst_ref=theirs.at[k - 1, source, :, :, span(chunk)],
             send_sem=pair_send.at[source, chunk, k - 1],
             recv_sem=pair_recv.at[source, chunk, k - 1],
@@ -1036,6 +1145,10 @@
         both = shares(source)
         for chunk in range(chunks):
             finish(source, chunk, both, index == planes - 1)
+    layer_ref[...] = (
+        mixed_ref[...].astype(jnp.float32)
+        + rms_scale(shared_ref[...] + out_ref[...], gain_ref[...])
+    ).astype(jnp.bfloat16)
     for index, source in enumerate(order):
         for chunk in range(chunks):
             for k in range(1, tp_count):
@@ -1046,10 +1159,10 @@
                 onward(source, chunk, 0, sp).wait_send()
 
 
-def combined_rows(dims, group, parts, marks):
+def combined_rows(dims, group, parts, marks, mixed, shared, gain):
     planes, rows, columns, tp_count = dims
     per_plane = rows * columns
-    padded, width = parts.shape[2:]
+    padded, width = parts.shape[3:]
     token_count = marks.shape[2]
     dma = pltpu.SemaphoreType.DMA
     block = (planes, per_plane, padded, width)
@@ -1057,10 +1170,11 @@
     chunks = math.gcd(width // 512, 2)
     return pl.pallas_call(
         functools.partial(combine_kernel, dims, group, chunks),
-        out_shape=jax.ShapeDtypeStruct((token_count, width), jnp.float32),
-        in_specs=[pl.BlockSpec(memory_space=pl.ANY), pl.BlockSpec(memory_space=pltpu.VMEM)],
+        out_shape=jax.ShapeDtypeStruct((token_count, width), jnp.bfloat16),
+        in_specs=[pl.BlockSpec(memory_space=pl.ANY)] + [pl.BlockSpec(memory_space=pltpu.VMEM)] * 4,
         out_specs=pl.BlockSpec(memory_space=pltpu.VMEM),
         scratch_shapes=[
+            pltpu.VMEM((token_count, width), jnp.float32),
             pltpu.VMEM(block, jnp.bfloat16),
             pltpu.VMEM((pairs,) + block, jnp.bfloat16),
             pltpu.VMEM(block, jnp.bfloat16),
@@ -1079,28 +1193,7 @@
             collective_id=2, has_side_effects=True, vmem_limit_bytes=56 * 1024 * 1024
         ),
         name="combine",
-    )(parts, marks)
-
-
-def run_experts(incoming, expert_gate, expert_up, expert_down, capacity):
-    sources = incoming.shape[0]
-    local_experts = expert_gate.shape[0]
-    grouped = incoming.reshape(sources, local_experts, capacity, D)
-    gate_part = jnp.einsum(
-        "rjcd,jdf->rjcf", grouped, expert_gate, preferred_element_type=jnp.float32
-    )
-    up_part = jnp.einsum("rjcd,jdf->rjcf", grouped, expert_up, preferred_element_type=jnp.float32)
-    hidden = (jax.nn.silu(gate_part) * up_part).astype(jnp.bfloat16)
-    result = jnp.stack(
-        [
-            jnp.einsum(
-                "rcf,fd->rcd", hidden[:, j], expert_down[j], preferred_element_type=jnp.float32
-            ).astype(jnp.bfloat16)
-            for j in range(local_experts)
-        ],
-        axis=1,
-    )
-    return result.reshape(sources, local_experts * capacity, D)
+    )(parts, marks, mixed, shared, gain.reshape(1, -1))
 
 
 def shards(
@@ -1154,35 +1247,30 @@
     local_experts = expert_gate.shape[0]
     experts_all = local_experts * sp_count
     capacity = max(2, 3 * row_count * TOPK // (2 * experts_all))
-    flat_ids = expert_ids.reshape(-1)
-    onehot = (flat_ids[:, None] == jnp.arange(experts_all, dtype=jnp.int32)[None, :]).astype(
-        jnp.int32
+    chosen = (
+        expert_ids[:, :, None] == jnp.arange(experts_all, dtype=jnp.int32)[None, None, :]
+    ).astype(jnp.float32)
+    named = jnp.sum(chosen, axis=1)
+    order = jnp.arange(row_count, dtype=jnp.int32)
+    earlier = jnp.dot(
+        (order[None, :] < order[:, None]).astype(jnp.bfloat16),
+        named.astype(jnp.bfloat16),
+        preferred_element_type=jnp.float32,
     )
-    earlier = jnp.cumsum(onehot, axis=0) - onehot
-    slot_rank = jnp.sum(earlier * onehot, axis=1)
-    slot_index = flat_ids * capacity + slot_rank
+    slot_rank = jnp.sum(chosen * earlier[:, None, :], axis=2).astype(jnp.int32)
+    slot_index = expert_ids * capacity + slot_rank
     group = local_experts * capacity
     dims = plane_shape(sp_count) + (tp_count,)
-    all_rows, marks = dispatched_rows(dims, group, normed, slot_index, route_weights)
-    padded = all_rows.shape[2]
-    partials = run_experts(
-        all_rows[:, :, :group].reshape(tp_count * sp_count, group, D),
-        expert_gate,
-        expert_up,
-        expert_down,
-        capacity,
+    parts, marks, shared_out = dispatched_rows(
+        dims,
+        group,
+        normed,
+        slot_index,
+        route_weights,
+        (expert_gate, expert_up, expert_down),
+        (shared_gate, shared_up, shared_down),
     )
-    partials = partials.astype(jnp.bfloat16).reshape(tp_count, sp_count, group, D)
-    if padded > group:
-        partials = jnp.pad(partials, ((0, 0), (0, 0), (0, padded - group), (0, 0)))
-    routed = combined_rows(dims, group, partials, marks)
-    shared_hidden = (
-        jax.nn.silu(jnp.dot(normed, shared_gate, preferred_element_type=jnp.float32))
-        * jnp.dot(normed, shared_up, preferred_element_type=jnp.float32)
-    ).astype(jnp.bfloat16)
-    shared_out = jnp.dot(shared_hidden, shared_down, preferred_element_type=jnp.float32)
-    combined = shared_out + routed
-    return (mixed_rows.astype(jnp.float32) + rms_scale(combined, gain_post)).astype(jnp.bfloat16)
+    return combined_rows(dims, group, parts, marks, mixed_rows, shared_out, gain_post)
 
 
 def solution(mesh):

time: 211 us -> 188 us (0.89)
  matrix products: 17.7 us -> 4.04 us
  Pallas kernels: 180 us -> 175 us
  local copies, waits for them, and re-layouts: 5.83 us -> 2.69 us
    dot_general x6 -> x1, matrix products: 13.7 us -> 0.14 us  [shards(): jnp.dot((order[None, :] < order[:, None]).astype(jnp.bfloat16), named.ast...]
    pallas_call x1, Pallas kernels: 94.3 us -> 83 us  [dispatched_rows(): pl.pallas_call(functools.partial(dispatch_kernel, dims, group, chunks), o...]
    pallas_call x1, Pallas kernels: 51 us -> 57.7 us  [combined_rows(): pl.pallas_call(functools.partial(combine_kernel, dims, group, chunks), ou...]
    another operation x2 -> x0, local copies, waits for them, and re-layouts: 3.24 us -> none  [the longest x1 3.24 us: run_experts(): jnp.stack([jnp.einsum('rcf,fd->rcd', hidden[:, j], expert_down[j], prefer...]
    convert_element_type x2 -> x0, other arithmetic: 2.26 us -> none  [the longest x1 2.25 us: shards(): (mixed_rows.astype(jnp.float32) + rms_scale(combined, gain_post)).astype(...]
where the time goes in v3:
time: 188 us; the launch traced here: 187 us
  Pallas kernels  175 us (93%)
  other arithmetic  5.65 us (3%)
  matrix products  4.04 us (2%)
  local copies, waits for them, and re-layouts  2.69 us (1%)
    pallas_call x1, Pallas kernels, dispatched_rows(): pl.pallas_call(functools.partial(dispatch_kernel, dims, group, chunks), o...  83 us
    pallas_call x1, Pallas kernels, combined_rows(): pl.pallas_call(functools.partial(combine_kernel, dims, group, chunks), ou...  57.7 us
    pallas_call x1, Pallas kernels, attended_rows(): pl.pallas_call(functools.partial(attend_kernel, (planes, rows, columns, t...  34.3 us

profile of v3, /device:TPU:0, one launch (start us, length us, event | category | flops | bytes accessed | tf_op | source)
XLA Modules:
  0.0 187.4 jit_solution(2755686562759354663)
XLA Ops:
  0.0 0.0 copy-start.1
  0.0 0.9 fusion.5
  0.9 0.7 broadcast_in_dim.2.lam_ref
  1.6 0.7 convert_reduce_fusion
  2.3 0.1 fusion.3
  2.4 0.7 select_reduce_fusion
  3.1 0.7 add_convert_fusion.1
  3.8 1.3 maximum_bitcast_fusion.slots_ref
  5.1 34.3 %gather_attend.1 = (bf16[128,1024]{1,0:T(8,128)(2,1)}, bf16[128,1024]{1,0:T(8,128)(2,1)}) custom-call(bf16[256,512]{1,0:T(8,128)(2,1)} %qn_ref.1, bf16[256,128]{1,0:T(8,128)(2,1)} %kn_ref.1, bf16[256,128]{1,0:T(8,128)(2,1)} %vn_ref.1, bf16[256,512]{1,0:T(8,128)(2,1)} %qw_ref.1, bf16[256,256]{1,0:T(8,128)(2,1)} %kw_ref.1, bf16[256,256]{1,0:T(8,128)(2,1)} %vw_ref.1, ...), custom_call_target="tpu_custom_call" | custom-call | tf_op jit(solution)/shard_map/gather_attend/pallas_call | solution.py:585
  39.4 0.0 copy-start.3
  39.4 3.0 %fusion.6 = f32[128,2048]{1,0:T(8,128)S(1)} fusion(bf16[128,1024]{1,0:T(8,128)(2,1)} %get-tuple-element.10, bf16[1024,2048]{1,0:T(8,128)(2,1)} %param.34), kind=kOutput, calls=%fused_computation.21 | convolution fusion | flops 536870912 | bytes 5505024 | tf_op jit(solution)/shard_map/dot_general | solution.py:1240
  42.4 0.0 copy-done.1
  42.4 0.0 copy-done.3
  42.4 0.0 copy-start.2
  42.4 0.0 copy-start.4
  42.4 0.0 copy-start.5
  42.5 0.9 multiply_reduce_fusion
  43.3 0.1 copy-done.2
  43.5 0.0 copy-done.4
  43.5 0.4 fusion
  43.8 0.0 copy-start
  43.9 0.0 copy-done.5
  43.9 1.0 fusion.2.normed_ref
  44.9 83.0 %dispatch.1 = (bf16[4,2,4,48,2048]{4,3,2,1,0:T(8,128)(2,1)}, f32[4,8,128]{2,1,0:T(8,128)}, f32[128,2048]{1,0:T(8,128)}) custom-call(bf16[128,2048]{1,0:T(8,128)(2,1)} %fusion.2.normed_ref, f32[8,128]{1,0:T(8,128)} %maximum_bitcast_fusion.slots_ref, bf16[2,2048,256]{2,1,0:T(8,128)(2,1)} %gate_ref.1, bf16[2,2048,256]{2,1,0:T(8,128)(2,1)} %up_ref.1, ...), custom_call_target="tpu_custom_call" | custom-call | tf_op jit(solution)/shard_map/dispatch/pallas_call | solution.py:936
  127.8 0.0 copy-done
  127.8 57.7 %combine.1 = bf16[128,2048]{1,0:T(8,128)(2,1)} custom-call(bf16[4,2,4,48,2048]{4,3,2,1,0:T(8,128)(2,1)} %get-tuple-element.12.parts_ref, f32[4,8,128]{2,1,0:T(8,128)} %get-tuple-element.13.marks_ref, bf16[128,2048]{1,0:T(8,128)(2,1)} %copy-done, f32[128,2048]{1,0:T(8,128)} %get-tuple-element.14.shared_ref, f32[1,2048]{1,0:T(1,128)} %bitcast.10), custom_call_target="tpu_custom_call" | custom-call | tf_op jit(solution)/shard_map/combine/pallas_call | solution.py:1171
  185.5 1.9 %copy.28 = bf16[128,2048]{1,0:T(8,128)(2,1)} copy(bf16[128,2048]{1,0:T(8,128)(2,1)} %combine.1) | data formatting | bytes 1048576
  (2 shorter events, 0.0 us)
Async XLA Ops:
  0.0 42.4 %copy-start.1 = (bf16[1024,2048]{1,0:T(8,128)(2,1)S(1)}, bf16[1024,2048]{1,0:T(8,128)(2,1)}, u32[]{:S(2)}) copy-start(bf16[1024,2048]{1,0:T(8,128)(2,1)} %param.35) | copy-start | bytes 12582916
  39.4 3.1 %copy-start.3 = (bf16[128,1024]{1,0:T(8,128)(2,1)S(1)}, bf16[128,1024]{1,0:T(8,128)(2,1)}, u32[]{:S(2)}) copy-start(bf16[128,1024]{1,0:T(8,128)(2,1)} %get-tuple-element.11) | copy-start | bytes 786436
  42.4 1.0 copy-start.2
  42.4 1.0 copy-start.4
  42.4 1.4 copy-start.5
  43.8 84.0 %copy-start = (bf16[128,2048]{1,0:T(8,128)(2,1)}, bf16[128,2048]{1,0:T(8,128)(2,1)S(1)}, u32[]{:S(2)}) copy-start(bf16[128,2048]{1,0:T(8,128)(2,1)S(1)} %get-tuple-element.16.mixed_ref) | copy-start | bytes 1572868

commit v4 on v3

--- a/solution.py
+++ b/solution.py
@@ -45,7 +45,8 @@
     qw_ref,
     kw_ref,
     vw_ref,
-    lam_ref,
+    lamn_ref,
+    lamw_ref,
     gainn_ref,
     gainw_ref,
     outn_ref,
@@ -62,6 +63,7 @@
     acc_n,
     acc_w,
     lam,
+    lam_own,
     load_sem,
     query_sem,
     query_recv,
@@ -95,6 +97,12 @@
     at_home = side == tp
     away = side != tp
 
+    weights = [lamn_ref[head] for head in range(lamn_ref.shape[0])]
+    weights += [lamw_ref[head] for head in range(lamw_ref.shape[0])]
+    lam_own[...] = jnp.zeros_like(lam_own)
+    for index, weight in enumerate(weights):
+        lam_own[index : index + 1, :] = jnp.full((1, lam_own.shape[1]), weight)
+
     def loads(into):
         copies = []
         begin = 0
@@ -106,28 +114,26 @@
             begin += width
         return copies
 
-    def query_loads():
-        return [
-            pltpu.make_async_copy(qn_ref, raw_n, query_sem.at[0]),
-            pltpu.make_async_copy(qw_ref, raw_w, query_sem.at[1]),
-        ]
-
-    def query_swaps():
-        return [
-            pltpu.make_async_remote_copy(
-                src_ref=source,
-                dst_ref=target,
-                send_sem=query_sem.at[index],
-                recv_sem=query_recv.at[index],
-                device_id={"sp": across_sp, "tp": 1 - tp},
-                device_id_type=MESH,
-            )
-            for index, (source, target) in enumerate(((qn_ref, raw_n), (qw_ref, raw_w)))
-        ]
+    moved = ((qn_ref, raw_n), (qw_ref, raw_w))
+
+    def query_load(index):
+        source, target = moved[index]
+        return pltpu.make_async_copy(source, target, query_sem.at[index])
+
+    def query_swap(index):
+        source, target = moved[index]
+        return pltpu.make_async_remote_copy(
+            src_ref=source,
+            dst_ref=target,
+            send_sem=query_sem.at[index],
+            recv_sem=query_recv.at[index],
+            device_id={"sp": across_sp, "tp": 1 - tp},
+            device_id_type=MESH,
+        )
 
     @pl.when(at_home)
     def _():
-        for copy in loads(kv.at[0, cell]) + query_loads():
+        for copy in loads(kv.at[0, cell]) + [query_load(0), query_load(1)]:
             copy.start()
 
     @pl.when(away)
@@ -265,7 +271,7 @@
             arrived(depth, peer(k) + 1 - 2 * side, 1 - tp)
 
     lam_copy = pltpu.make_async_remote_copy(
-        src_ref=lam_ref,
+        src_ref=lam_own,
         dst_ref=lam,
         send_sem=lam_sem.at[0],
         recv_sem=lam_sem.at[1],
@@ -280,13 +286,13 @@
         for copy in whole_copies():
             copy.start()
         lam_copy.start()
-        lam[...] = lam_ref[...]
+        lam[...] = lam_own[...]
 
     @pl.when(away)
     def _():
         for copy in loads(own):
             copy.wait()
-        for copy in swap_copies() + query_swaps():
+        for copy in swap_copies() + [query_swap(0), query_swap(1)]:
             copy.start()
         arrived(0, cell, tp)
 
@@ -323,7 +329,7 @@
         row_max[state] = jnp.broadcast_to(now, row_max.shape[1:])
         row_sum[state] = jnp.broadcast_to(total, row_sum.shape[1:])
 
-    def attend(depth, masked):
+    def attend(depth, masked, group):
         def part(at):
             def columns_of(begin, width):
                 return kv[depth, pl.ds(at, chunk), :, begin : begin + width].reshape(
@@ -371,8 +377,10 @@
                     )
                 return carry
 
-            lax.fori_loop(0, heads_n, narrow, 0)
-            lax.fori_loop(0, heads_w, wide, 0)
+            if group == 0:
+                lax.fori_loop(0, heads_n, narrow, 0)
+            else:
+                lax.fori_loop(0, heads_w, wide, 0)
 
         if per_plane == chunk:
             part(0)
@@ -383,67 +391,12 @@
                 return carry
 
             lax.fori_loop(0, per_plane // chunk, step, 0)
-
-    arrived(0, across, tp)
-    spread(0, 1)
-    pair_copy(0, 1).start()
-    relay(0)
-
-    @pl.when(plane > 0)
-    def _():
-        line(1)
-
-    @pl.when(at_home)
-    def _():
-        for copy in query_loads():
-            copy.wait()
-
-    @pl.when(away)
-    def _():
-        for copy in query_swaps():
-            copy.wait()
-
-    for head in range(heads_n):
-        both = raw_n[:, head * width_k : (head + 1) * width_k]
-        lane = lax.broadcasted_iota(jnp.int32, both.shape, 1)
-        zero = jnp.zeros_like(both)
-        maps_n[head, 0] = jnp.where(lane < DN, both, zero)
-        maps_n[head, 1] = jnp.where(lane < DN, zero, both)
-
-    @pl.when(away)
-    def _():
-        arrived(0, cell, 1 - tp)
-        lam_copy.wait_recv()
-
-    arrived(0, across, 1 - tp)
-    finish(0)
-    attend(0, True)
-
-    def depth_step(depth, carry):
-        relay(depth)
-
-        @pl.when(depth < plane)
-        def _():
-            line(depth + 1)
-
-        arrived(depth, cell, 1 - tp)
-        arrived(depth, across, 1 - tp)
-        finish(depth)
-        attend(depth, False)
-        return carry
-
-    lax.fori_loop(1, plane + 1, depth_step, 0)
 
     def close(first, second, weight, gain):
         head = first - weight * second
         scale = lax.rsqrt(jnp.mean(head * head, axis=1, keepdims=True) + EPS)
         return (head * scale * gain).astype(jnp.bfloat16)
 
-    for head in range(heads_n):
-        maps = [acc_n[2 * head + k] / row_sum[2 * head + k][:, :1] for k in range(2)]
-        att_n[:, head * value_n : (head + 1) * value_n] = close(
-            maps[0], maps[1], lam[head : head + 1, :1], gainn_ref[...]
-        )
     share = outn_ref.shape[0]
     home_sp = plane * per_plane + query_cell
 
@@ -498,7 +451,78 @@
             device_id_type=MESH,
         ).wait_recv()
 
-    send_out(0, start)
+    def close_narrow():
+        for head in range(heads_n):
+            maps = [acc_n[2 * head + k] / row_sum[2 * head + k][:, :1] for k in range(2)]
+            att_n[:, head * value_n : (head + 1) * value_n] = close(
+                maps[0], maps[1], lam[head : head + 1, :1], gainn_ref[...]
+            )
+        send_out(0, start)
+
+    arrived(0, across, tp)
+    spread(0, 1)
+    pair_copy(0, 1).start()
+    relay(0)
+
+    @pl.when(plane > 0)
+    def _():
+        line(1)
+
+    def query_wait(index):
+        @pl.when(at_home)
+        def _():
+            query_load(index).wait()
+
+        @pl.when(away)
+        def _():
+            query_swap(index).wait()
+
+    query_wait(0)
+
+    for head in range(heads_n):
+        both = raw_n[:, head * width_k : (head + 1) * width_k]
+        lane = lax.broadcasted_iota(jnp.int32, both.shape, 1)
+        zero = jnp.zeros_like(both)
+        maps_n[head, 0] = jnp.where(lane < DN, both, zero)
+        maps_n[head, 1] = jnp.where(lane < DN, zero, both)
+
+    @pl.when(away)
+    def _():
+        arrived(0, cell, 1 - tp)
+        lam_copy.wait_recv()
+
+    arrived(0, across, 1 - tp)
+    finish(0)
+    attend(0, True, 0)
+
+    @pl.when(plane == 0)
+    def _():
+        close_narrow()
+
+    query_wait(1)
+    attend(0, True, 1)
+
+    def depth_step(depth, carry):
+        relay(depth)
+
+        @pl.when(depth < plane)
+        def _():
+            line(depth + 1)
+
+        arrived(depth, cell, 1 - tp)
+        arrived(depth, across, 1 - tp)
+        finish(depth)
+        attend(depth, False, 0)
+
+        @pl.when(depth == plane)
+        def _():
+            close_narrow()
+
+        attend(depth, False, 1)
+        return carry
+
+    lax.fori_loop(1, plane + 1, depth_step, 0)
+
     for head in range(heads_w):
         maps = [
             acc_w[2 * head + k] / row_sum[2 * (heads_n + head) + k][:, :1] for k in range(2)
@@ -577,9 +601,8 @@
     tiles = 2 * (heads_n + heads_w)
     share = count // tp_count
     vmem = pl.BlockSpec(memory_space=pltpu.VMEM)
-    lambdas = jnp.concatenate([lambda_narrow, lambda_wide])
-    lambdas = jnp.pad(lambdas, (0, -lambdas.shape[0] % 8))
-    lambdas = jnp.broadcast_to(lambdas[:, None], (lambdas.shape[0], 128))
+    smem = pl.BlockSpec(memory_space=pltpu.SMEM)
+    lambdas = (-(-(heads_n + heads_w) // 8) * 8, 128)
     hbm = pl.BlockSpec(memory_space=pl.ANY)
     dma = pltpu.SemaphoreType.DMA
     return pl.pallas_call(
@@ -588,7 +611,7 @@
             jax.ShapeDtypeStruct((share, tp_count * heads_n * VN), jnp.bfloat16),
             jax.ShapeDtypeStruct((share, tp_count * heads_w * VW), jnp.bfloat16),
         ],
-        in_specs=[hbm, hbm, hbm, hbm, hbm, hbm, vmem, vmem, vmem],
+        in_specs=[hbm, hbm, hbm, hbm, hbm, hbm, smem, smem, vmem, vmem],
         out_specs=[vmem, vmem],
         scratch_shapes=[
             pltpu.VMEM((planes, per_plane, count, width), jnp.bfloat16),
@@ -602,7 +625,8 @@
             pltpu.VMEM((tiles, count, 128), jnp.float32),
             pltpu.VMEM((2 * heads_n, count, VN), jnp.float32),
             pltpu.VMEM((2 * heads_w, count, VW), jnp.float32),
-            pltpu.VMEM(lambdas.shape, jnp.float32),
+            pltpu.VMEM(lambdas, jnp.float32),
+            pltpu.VMEM(lambdas, jnp.float32),
             dma((4,)),
             dma((2,)),
             dma((2,)),
@@ -628,7 +652,8 @@
         queries_wide,
         keys_wide,
         values_wide,
-        lambdas,
+        lambda_narrow,
+        lambda_wide,
         gain_narrow.reshape(1, -1),
         gain_wide.reshape(1, -1),
     )
@@ -667,7 +692,7 @@
     return values / (1.0 + jnp.exp(-values))
 
 
-def dispatch_kernel(
+def expert_kernel(
     dims,
     group,
     chunks,
@@ -679,13 +704,20 @@
     shared_gate_ref,
     shared_up_ref,
     shared_down_ref,
-    parts,
+    mixed_ref,
+    gain_ref,
+    layer_ref,
     marks,
     shared_out,
+    summed,
     held,
     stage,
     inbox,
     result,
+    theirs,
+    back,
+    leaving,
+    landed,
     gate,
     up,
     down,
@@ -702,7 +734,12 @@
     cell_send,
     pair_recv,
     pair_send,
-    store_sem,
+    part_recv,
+    part_send,
+    back_recv,
+    back_send,
+    far_recv,
+    far_send,
 ):
     planes, rows, columns, tp_count = dims
     per_plane = rows * columns
@@ -792,8 +829,47 @@
             device_id_type=MESH,
         )
 
-    def store(source):
-        return pltpu.make_async_copy(result.at[source], parts.at[source], store_sem.at[source])
+    def part_copy(source, chunk, k):
+        other = (tp + k) % tp_count
+        return pltpu.make_async_remote_copy(
+            src_ref=result.at[source, other, :, :, span(chunk)],
+            dst_ref=theirs.at[k - 1, source, :, :, span(chunk)],
+            send_sem=part_send.at[source, chunk, k - 1],
+            recv_sem=part_recv.at[source, chunk, k - 1],
+            device_id={"tp": other},
+            device_id_type=MESH,
+        )
+
+    def back_to(source, chunk, k):
+        other = (cell + k) % per_plane
+        return pltpu.make_async_remote_copy(
+            src_ref=stage.at[source, other, :, span(chunk)],
+            dst_ref=back.at[source, cell, :, span(chunk)],
+            send_sem=back_send.at[source, chunk, k],
+            recv_sem=back_recv.at[source, chunk, (per_plane - k) % per_plane],
+            device_id={"sp": plane * per_plane + other},
+            device_id_type=MESH,
+        )
+
+    def back_from(source, chunk, k):
+        return pltpu.make_async_remote_copy(
+            src_ref=stage.at[source, cell, :, span(chunk)],
+            dst_ref=back.at[source, (cell + k) % per_plane, :, span(chunk)],
+            send_sem=back_send.at[source, chunk, k],
+            recv_sem=back_recv.at[source, chunk, k],
+            device_id={"sp": sp},
+            device_id_type=MESH,
+        )
+
+    def homeward(source, chunk, way, target):
+        return pltpu.make_async_remote_copy(
+            src_ref=leaving.at[source, :, span(chunk)],
+            dst_ref=landed.at[way, source, :, span(chunk)],
+            send_sem=far_send.at[source, chunk],
+            recv_sem=far_recv.at[way, source, chunk],
+            device_id={"sp": target},
+            device_id_type=MESH,
+        )
 
     def onward(source, act):
         @pl.when((source <= plane) & (plane < planes - 1))
@@ -804,35 +880,37 @@
         def _():
             act(1, sp - per_plane)
 
-    def body(source, first):
-        if not first:
-            mark_hop(source, 0, sp).wait_recv()
+    def forward(source, chunk):
+        onward(source, lambda way, target: row_hop(source, chunk, way, target).start())
+
+    def arrive(source):
+        mark_hop(source, 0, sp).wait_recv()
         onward(source, lambda way, target: mark_hop(source, way, target).start())
+        for chunk in range(chunks):
+            row_hop(source, chunk, 0, sp).wait_recv()
+            forward(source, chunk)
+
+    def select(source):
         slots = marks[source]
         row = lax.broadcasted_iota(jnp.int32, (padded, token_count), 0)
+        picks = []
+        for k in list(range(1, per_plane)) + [0]:
+            base = (plane * per_plane + (cell + k) % per_plane) * group
+            wanted = jnp.where(row < group, row + base, -1).astype(jnp.float32)
+            hit = slots[0:1, :] == wanted
+            for choice in range(1, TOPK):
+                hit = hit | (slots[choice : choice + 1, :] == wanted)
+            picks.append((k, jnp.where(hit, 1.0, 0.0).astype(jnp.bfloat16)))
         for chunk in range(chunks):
-            if not first:
-                row_hop(source, chunk, 0, sp).wait_recv()
-            onward(
-                source, lambda way, target: row_hop(source, chunk, way, target).start()
-            )
             tokens = held[source, :, span(chunk)]
-            for k in list(range(1, per_plane)) + [0]:
-                other = (cell + k) % per_plane
-                base = (plane * per_plane + other) * group
-                wanted = jnp.where(row < group, row + base, -1).astype(jnp.float32)
-                hit = slots[0:1, :] == wanted
-                for choice in range(1, TOPK):
-                    hit = hit | (slots[choice : choice + 1, :] == wanted)
-                chosen = jnp.dot(
-                    jnp.where(hit, 1.0, 0.0).astype(jnp.bfloat16),
-                    tokens,
-                    preferred_element_type=jnp.float32,
-                ).astype(jnp.bfloat16)
+            for k, pick in picks:
+                chosen = jnp.dot(pick, tokens, preferred_element_type=jnp.float32).astype(
+                    jnp.bfloat16
+                )
                 if k == 0:
                     inbox[source, tp, cell, :, span(chunk)] = chosen
                 else:
-                    stage[source, other, :, span(chunk)] = chosen
+                    stage[source, (cell + k) % per_plane, :, span(chunk)] = chosen
                     to_cell(source, chunk, k).start()
 
     def finish(source):
@@ -873,9 +951,85 @@
             if end > begin + both:
                 result[source, :, :, begin + both : end, :] = out[:, :, both:]
             done = max(done, end)
-        store(source).start()
-
-    body(plane, True)
+        for chunk in range(chunks):
+            for k in range(1, tp_count):
+                part_copy(source, chunk, k).start()
+
+    def hand_back(source):
+        for chunk in range(chunks):
+            for k in range(1, per_plane):
+                to_cell(source, chunk, k).wait_send()
+            for k in range(1, tp_count):
+                part_copy(source, chunk, k).wait_recv()
+            for k in list(range(1, per_plane)) + [0]:
+                other = (cell + k) % per_plane
+                total = result[source, tp, other, :, span(chunk)].astype(jnp.float32)
+                for i in range(tp_count - 1):
+                    total += theirs[i, source, other, :, span(chunk)].astype(jnp.float32)
+                if k == 0:
+                    back[source, cell, :, span(chunk)] = total.astype(jnp.bfloat16)
+                else:
+                    stage[source, other, :, span(chunk)] = total.astype(jnp.bfloat16)
+                    back_to(source, chunk, k).start()
+
+    def gather_up(source, last):
+        slots = marks[source]
+        row = lax.broadcasted_iota(jnp.int32, (per_plane * padded, token_count), 0)
+        block = lax.div(row, padded)
+        inner = row - block * padded
+        wanted = jnp.where(
+            inner < group, inner + (plane * per_plane + block) * group, -1
+        ).astype(jnp.float32)
+        share = jnp.zeros(wanted.shape, jnp.float32)
+        for choice in range(TOPK):
+            share += jnp.where(
+                slots[choice : choice + 1, :] == wanted,
+                slots[TOPK + choice : TOPK + choice + 1, :],
+                0.0,
+            )
+        coarse = share.astype(jnp.bfloat16)
+        fine = (share - coarse.astype(jnp.float32)).astype(jnp.bfloat16)
+        both = jnp.concatenate([coarse, fine], axis=1)
+        if last:
+            comes = [(0, plane > 0), (1, plane < planes - 1)]
+        else:
+            ahead = source > plane
+            behind = source < plane
+            comes = [(0, ahead & (plane > 0)), (1, behind & (plane < planes - 1))]
+        for chunk in range(chunks):
+            for k in range(1, per_plane):
+                back_from(source, chunk, k).wait_recv()
+            begin = chunk * wide
+            for at in range(begin, begin + wide, 512):
+                values = back[source, :, :, at : at + 512].reshape(per_plane * padded, 512)
+                pieces = lax.dot_general(
+                    both, values, (((0,), (0,)), ((), ())), preferred_element_type=jnp.float32
+                )
+                summed[:, at : at + 512] = pieces[:token_count] + pieces[token_count:]
+            for way, exists in comes:
+
+                @pl.when(exists)
+                def _(way=way, chunk=chunk):
+                    homeward(source, chunk, way, sp).wait_recv()
+                    summed[:, span(chunk)] += landed[way, source, :, span(chunk)].astype(
+                        jnp.float32
+                    )
+
+            if not last:
+                leaving[source, :, span(chunk)] = summed[:, span(chunk)].astype(jnp.bfloat16)
+
+                @pl.when(ahead)
+                def _(chunk=chunk):
+                    homeward(source, chunk, 0, sp + per_plane).start()
+
+                @pl.when(behind)
+                def _(chunk=chunk):
+                    homeward(source, chunk, 1, sp - per_plane).start()
+
+    onward(plane, lambda way, target: mark_hop(plane, way, target).start())
+    for chunk in range(chunks):
+        forward(plane, chunk)
+    select(plane)
     for copy in weights[:3]:
         copy.wait()
     normed = held[plane]
@@ -888,18 +1042,68 @@
     for copy in weights[3:]:
         copy.wait()
 
-    def step(_, carry):
-        low, high, before = carry
-        use_high = (low < 0) | ((high < planes) & (high - plane <= plane - low))
+    at_edge = (plane == 0) | (plane == planes - 1)
+    first_out = jnp.where(plane == 0, 1, planes - 2)
+
+    finish(plane)
+    experts(plane)
+
+    def process(source):
+        finish(source)
+        experts(source)
+        hand_back(source)
+
+    def each(distance, act):
+        def one(side, carry):
+            source = plane + (2 * side - 1) * distance
+
+            @pl.when((source >= 0) & (source < planes))
+            def _():
+                act(source)
+
+            return carry
+
+        lax.fori_loop(0, 2, one, 0)
+
+    def step(distance, carry):
+        each(distance, arrive)
+        each(distance, select)
+
+        @pl.when(distance > 1)
+        def _():
+            each(distance - 1, process)
+
+        return carry
+
+    lax.fori_loop(1, planes, step, 0)
+
+    @pl.when(at_edge & (planes > 2))
+    def _():
+        gather_up(first_out, False)
+
+    each(planes - 1, process)
+    hand_back(plane)
+
+    def chain(index, carry):
+        low, high = carry
+        use_high = (low < 0) | (
+            (high < planes)
+            & (2 * high + plane <= 2 * (planes - 1 - low) + (planes - 1 - plane))
+        )
         source = jnp.where(use_high, high, low)
-        body(source, False)
-        finish(before)
-        experts(before)
-        return jnp.where(use_high, low, low - 1), jnp.where(use_high, high + 1, high), source
-
-    last = lax.fori_loop(0, planes - 1, step, (plane - 1, plane + 1, plane))[2]
-    finish(last)
-    experts(last)
+
+        @pl.when(jnp.logical_not(at_edge & (index == 0) & (planes > 2)))
+        def _():
+            gather_up(source, False)
+
+        return jnp.where(use_high, low, low - 1), jnp.where(use_high, high + 1, high)
+
+    lax.fori_loop(0, planes - 1, chain, (plane - 1, plane + 1))
+    gather_up(plane, True)
+    layer_ref[...] = (
+        mixed_ref[...].astype(jnp.float32)
+        + rms_scale(shared_out[...] + summed[...], gain_ref[...])
+    ).astype(jnp.bfloat16)
 
     def drain(source, carry):
         onward(source, lambda way, target: mark_hop(source, way, target).wait_send())
@@ -908,17 +1112,30 @@
                 source, lambda way, target: row_hop(source, chunk, way, target).wait_send()
             )
             for k in range(1, per_plane):
-                to_cell(source, chunk, k).wait_send()
+                back_to(source, chunk, k).wait_send()
             for k in range(1, tp_count):
                 to_pair(source, chunk, k).wait_send()
-        store(source).wait()
+                part_copy(source, chunk, k).wait_send()
+
+            @pl.when(source != plane)
+            def _():
+                homeward(source, chunk, 0, sp).wait_send()
+
         return carry
 
     lax.fori_loop(0, planes, drain, 0)
 
 
-def dispatched_rows(
-    dims, group, normed, slot_index, route_weights, routed_weights, shared_weights
+def expert_rows(
+    dims,
+    group,
+    normed,
+    slot_index,
+    route_weights,
+    routed_weights,
+    shared_weights,
+    mixed,
+    gain,
 ):
     planes, rows, columns, tp_count = dims
     per_plane = rows * columns
@@ -929,24 +1146,28 @@
     hbm = pl.BlockSpec(memory_space=pl.ANY)
     vmem = pl.BlockSpec(memory_space=pltpu.VMEM)
     dma = pltpu.SemaphoreType.DMA
-    chunks = math.gcd(width // 512, 2)
+    chunks = math.gcd(width // 512, 4)
     pairs = max(1, tp_count - 1)
     weights = list(routed_weights) + list(shared_weights)
+    block = (planes, per_plane, padded, width)
     inbox = (planes, tp_count, per_plane, padded, width)
     return pl.pallas_call(
-        functools.partial(dispatch_kernel, dims, group, chunks),
-        out_shape=[
-            jax.ShapeDtypeStruct(inbox, jnp.bfloat16),
-            jax.ShapeDtypeStruct((planes, 2 * TOPK, token_count), jnp.float32),
-            jax.ShapeDtypeStruct((token_count, width), jnp.float32),
-        ],
-        in_specs=[hbm] * (2 + len(weights)),
-        out_specs=[hbm, vmem, vmem],
+        functools.partial(expert_kernel, dims, group, chunks),
+        out_shape=jax.ShapeDtypeStruct((token_count, width), jnp.bfloat16),
+        in_specs=[hbm] * (2 + len(weights)) + [vmem, vmem],
+        out_specs=vmem,
         scratch_shapes=[
+            pltpu.VMEM((planes, 2 * TOPK, token_count), jnp.float32),
+            pltpu.VMEM((token_count, width), jnp.float32),
+            pltpu.VMEM((token_count, width), jnp.float32),
             pltpu.VMEM((planes, token_count, width), jnp.bfloat16),
-            pltpu.VMEM((planes, per_plane, padded, width), jnp.bfloat16),
+            pltpu.VMEM(block, jnp.bfloat16),
             pltpu.VMEM(inbox, jnp.bfloat16),
             pltpu.VMEM(inbox, jnp.bfloat16),
+            pltpu.VMEM((pairs,) + block, jnp.bfloat16),
+            pltpu.VMEM(block, jnp.bfloat16),
+            pltpu.VMEM((planes, token_count, width), jnp.bfloat16),
+            pltpu.VMEM((2, planes, token_count, width), jnp.bfloat16),
         ]
         + [pltpu.VMEM(weight.shape, jnp.bfloat16) for weight in weights]
         + [
@@ -960,228 +1181,6 @@
             dma((planes, chunks, per_plane)),
             dma((planes, chunks, pairs)),
             dma((planes, chunks, pairs)),
-            dma((planes,)),
-        ],
-        compiler_params=pltpu.CompilerParams(
-            collective_id=1, has_side_effects=True, vmem_limit_bytes=60 * 1024 * 1024
-        ),
-        name="dispatch",
-    )(normed, slots, *weights)
-
-
-def combine_kernel(
-    dims,
-    group,
-    chunks,
-    parts_ref,
-    marks_ref,
-    mixed_ref,
-    shared_ref,
-    gain_ref,
-    layer_ref,
-    out_ref,
-    mine,
-    theirs,
-    stage,
-    back,
-    leaving,
-    landed,
-    load_sem,
-    pair_recv,
-    pair_send,
-    cell_recv,
-    cell_send,
-    far_recv,
-    far_send,
-):
-    planes, rows, columns, tp_count = dims
-    per_plane = rows * columns
-    plane, cell, sp, tp = plane_greeting(planes, rows, columns, tp_count)
-    padded = stage.shape[2]
-    token_count = out_ref.shape[0]
-
-    order = []
-    low, high = jnp.int32(0), jnp.int32(planes - 1)
-    for _ in range(planes - 1):
-        use_high = high - plane >= plane - low
-        order.append(jnp.where(use_high, high, low))
-        high = jnp.where(use_high, high - 1, high)
-        low = jnp.where(use_high, low, low + 1)
-    order.append(plane)
-
-    wide = out_ref.shape[1] // chunks
-
-    def span(chunk):
-        return pl.ds(chunk * wide, wide)
-
-    def load(source, chunk):
-        return pltpu.make_async_copy(
-            parts_ref.at[source, tp, :, :, span(chunk)],
-            mine.at[source, :, :, span(chunk)],
-            load_sem.at[source, chunk],
-        )
-
-    def to_pair(source, chunk, k):
-        other = (tp + k) % tp_count
-        return pltpu.make_async_remote_copy(
-            src_ref=parts_ref.at[source, other, :, :, span(chunk)],
-            dst_ref=theirs.at[k - 1, source, :, :, span(chunk)],
-            send_sem=pair_send.at[source, chunk, k - 1],
-            recv_sem=pair_recv.at[source, chunk, k - 1],
-            device_id={"tp": other},
-            device_id_type=MESH,
-        )
-
-    def to_cell(source, chunk, k):
-        other = (cell + k) % per_plane
-        return pltpu.make_async_remote_copy(
-            src_ref=stage.at[source, other, :, span(chunk)],
-            dst_ref=back.at[source, cell, :, span(chunk)],
-            send_sem=cell_send.at[source, chunk, k],
-            recv_sem=cell_recv.at[source, chunk, (per_plane - k) % per_plane],
-            device_id={"sp": plane * per_plane + other},
-            device_id_type=MESH,
-        )
-
-    def from_cell(source, chunk, k):
-        return pltpu.make_async_remote_copy(
-            src_ref=stage.at[source, cell, :, span(chunk)],
-            dst_ref=back.at[source, (cell + k) % per_plane, :, span(chunk)],
-            send_sem=cell_send.at[source, chunk, k],
-            recv_sem=cell_recv.at[source, chunk, k],
-            device_id={"sp": sp},
-            device_id_type=MESH,
-        )
-
-    def onward(source, chunk, way, target):
-        return pltpu.make_async_remote_copy(
-            src_ref=leaving.at[source, :, span(chunk)],
-            dst_ref=landed.at[way, source, :, span(chunk)],
-            send_sem=far_send.at[source, chunk],
-            recv_sem=far_recv.at[way, source, chunk],
-            device_id={"sp": target},
-            device_id_type=MESH,
-        )
-
-    items = [(source, chunk) for source in order for chunk in range(chunks)]
-    for item in items:
-        load(*item).start()
-        for k in range(1, tp_count):
-            to_pair(*item, k).start()
-
-    def body(source, chunk):
-        load(source, chunk).wait()
-        for k in range(1, tp_count):
-            to_pair(source, chunk, k).wait_recv()
-        for k in list(range(1, per_plane)) + [0]:
-            other = (cell + k) % per_plane
-            total = mine[source, other, :, span(chunk)].astype(jnp.float32)
-            for i in range(tp_count - 1):
-                total += theirs[i, source, other, :, span(chunk)].astype(jnp.float32)
-            if k == 0:
-                back[source, cell, :, span(chunk)] = total.astype(jnp.bfloat16)
-            else:
-                stage[source, other, :, span(chunk)] = total.astype(jnp.bfloat16)
-                to_cell(source, chunk, k).start()
-
-    def shares(source):
-        marks = marks_ref[source]
-        row = lax.broadcasted_iota(jnp.int32, (per_plane * padded, token_count), 0)
-        block = lax.div(row, padded)
-        inner = row - block * padded
-        wanted = jnp.where(
-            inner < group, inner + (plane * per_plane + block) * group, -1
-        ).astype(jnp.float32)
-        share = jnp.zeros(wanted.shape, jnp.float32)
-        for choice in range(TOPK):
-            share += jnp.where(
-                marks[choice : choice + 1, :] == wanted,
-                marks[TOPK + choice : TOPK + choice + 1, :],
-                0.0,
-            )
-        high = share.astype(jnp.bfloat16)
-        low = (share - high.astype(jnp.float32)).astype(jnp.bfloat16)
-        return jnp.concatenate([high, low], axis=1)
-
-    def finish(source, chunk, both, last):
-        for k in range(1, per_plane):
-            from_cell(source, chunk, k).wait_recv()
-        begin = chunk * wide
-        for at in range(begin, begin + wide, 512):
-            values = back[source, :, :, at : at + 512].reshape(per_plane * padded, 512)
-            pieces = lax.dot_general(
-                both, values, (((0,), (0,)), ((), ())), preferred_element_type=jnp.float32
-            )
-            out_ref[:, at : at + 512] = pieces[:token_count] + pieces[token_count:]
-        if last:
-            comes = [(0, plane > 0), (1, plane < planes - 1)]
-        else:
-            up = source > plane
-            comes = [
-                (0, up & (plane > 0)),
-                (1, jnp.logical_not(up) & (plane < planes - 1)),
-            ]
-        for way, exists in comes:
-
-            @pl.when(exists)
-            def _(way=way):
-                onward(source, chunk, way, sp).wait_recv()
-                out_ref[:, span(chunk)] += landed[way, source, :, span(chunk)].astype(jnp.float32)
-
-        if not last:
-            leaving[source, :, span(chunk)] = out_ref[:, span(chunk)].astype(jnp.bfloat16)
-
-            @pl.when(up)
-            def _():
-                onward(source, chunk, 0, sp + per_plane).start()
-
-            @pl.when(jnp.logical_not(up))
-            def _():
-                onward(source, chunk, 1, sp - per_plane).start()
-
-    for item in items:
-        body(*item)
-    for index, source in enumerate(order):
-        both = shares(source)
-        for chunk in range(chunks):
-            finish(source, chunk, both, index == planes - 1)
-    layer_ref[...] = (
-        mixed_ref[...].astype(jnp.float32)
-        + rms_scale(shared_ref[...] + out_ref[...], gain_ref[...])
-    ).astype(jnp.bfloat16)
-    for index, source in enumerate(order):
-        for chunk in range(chunks):
-            for k in range(1, tp_count):
-                to_pair(source, chunk, k).wait_send()
-            for k in range(1, per_plane):
-                to_cell(source, chunk, k).wait_send()
-            if index < planes - 1:
-                onward(source, chunk, 0, sp).wait_send()
-
-
-def combined_rows(dims, group, parts, marks, mixed, shared, gain):
-    planes, rows, columns, tp_count = dims
-    per_plane = rows * columns
-    padded, width = parts.shape[3:]
-    token_count = marks.shape[2]
-    dma = pltpu.SemaphoreType.DMA
-    block = (planes, per_plane, padded, width)
-    pairs = max(1, tp_count - 1)
-    chunks = math.gcd(width // 512, 2)
-    return pl.pallas_call(
-        functools.partial(combine_kernel, dims, group, chunks),
-        out_shape=jax.ShapeDtypeStruct((token_count, width), jnp.bfloat16),
-        in_specs=[pl.BlockSpec(memory_space=pl.ANY)] + [pl.BlockSpec(memory_space=pltpu.VMEM)] * 4,
-        out_specs=pl.BlockSpec(memory_space=pltpu.VMEM),
-        scratch_shapes=[
-            pltpu.VMEM((token_count, width), jnp.float32),
-            pltpu.VMEM(block, jnp.bfloat16),
-            pltpu.VMEM((pairs,) + block, jnp.bfloat16),
-            pltpu.VMEM(block, jnp.bfloat16),
-            pltpu.VMEM(block, jnp.bfloat16),
-            pltpu.VMEM((planes, token_count, width), jnp.bfloat16),
-            pltpu.VMEM((2, planes, token_count, width), jnp.bfloat16),
-            dma((planes, chunks)),
             dma((planes, chunks, pairs)),
             dma((planes, chunks, pairs)),
             dma((planes, chunks, per_plane)),
@@ -1190,10 +1189,10 @@
             dma((planes, chunks)),
         ],
         compiler_params=pltpu.CompilerParams(
-            collective_id=2, has_side_effects=True, vmem_limit_bytes=56 * 1024 * 1024
+            collective_id=1, has_side_effects=True, vmem_limit_bytes=60 * 1024 * 1024
         ),
-        name="combine",
-    )(parts, marks, mixed, shared, gain.reshape(1, -1))
+        name="expert_layer",
+    )(normed, slots, *weights, mixed, gain.reshape(1, -1))
 
 
 def shards(
@@ -1261,7 +1260,7 @@
     slot_index = expert_ids * capacity + slot_rank
     group = local_experts * capacity
     dims = plane_shape(sp_count) + (tp_count,)
-    parts, marks, shared_out = dispatched_rows(
+    return expert_rows(
         dims,
         group,
         normed,
@@ -1269,8 +1268,9 @@
         route_weights,
         (expert_gate, expert_up, expert_down),
         (shared_gate, shared_up, shared_down),
+        mixed_rows,
+        gain_post,
     )
-    return combined_rows(dims, group, parts, marks, mixed_rows, shared_out, gain_post)
 
 
 def solution(mesh):

time: 188 us -> 178 us (0.947)
  Pallas kernels: 175 us -> 169 us
  other arithmetic: 5.65 us -> 2.03 us
    pallas_call x2 -> x1, Pallas kernels: 141 us -> 137 us  [expert_rows(): pl.pallas_call(functools.partial(expert_kernel, dims, group, chunks), out...]
    pallas_call x1, Pallas kernels: 34.3 us -> 32.2 us  [attended_rows(): pl.pallas_call(functools.partial(attend_kernel, (planes, rows, columns, t...]
where the time goes in v4:
time: 178 us
  Pallas kernels  169 us (95%)
  matrix products  4.04 us (2%)
  other arithmetic  2.03 us (1%)
  local copies, waits for them, and re-layouts  2 us (1%)
    pallas_call x1, Pallas kernels, expert_rows(): pl.pallas_call(functools.partial(expert_kernel, dims, group, chunks), out...  137 us
    pallas_call x1, Pallas kernels, attended_rows(): pl.pallas_call(functools.partial(attend_kernel, (planes, rows, columns, t...  32.2 us

profile of v4, /device:TPU:0, one launch (start us, length us, event | category | flops | bytes accessed | tf_op | source)
XLA Modules:
  0.0 177.6 jit_solution(1187405967970314389)
XLA Ops:
  0.0 0.0 copy-start.1
  0.0 32.2 %gather_attend.1 = (bf16[128,1024]{1,0:T(8,128)(2,1)}, bf16[128,1024]{1,0:T(8,128)(2,1)}) custom-call(bf16[256,512]{1,0:T(8,128)(2,1)} %qn_ref.1, bf16[256,128]{1,0:T(8,128)(2,1)} %kn_ref.1, bf16[256,128]{1,0:T(8,128)(2,1)} %vn_ref.1, bf16[256,512]{1,0:T(8,128)(2,1)} %qw_ref.1, bf16[256,256]{1,0:T(8,128)(2,1)} %kw_ref.1, bf16[256,256]{1,0:T(8,128)(2,1)} %vw_ref.1, ...), custom_call_target="tpu_custom_call" | custom-call | tf_op jit(solution)/shard_map/gather_attend/pallas_call | solution.py:608
  32.2 0.0 copy-start.3
  32.2 3.0 %fusion.5 = f32[128,2048]{1,0:T(8,128)S(1)} fusion(bf16[128,1024]{1,0:T(8,128)(2,1)} %get-tuple-element.7, bf16[1024,2048]{1,0:T(8,128)(2,1)} %param.34), kind=kOutput, calls=%fused_computation.18 | convolution fusion | flops 536870912 | bytes 5505024 | tf_op jit(solution)/shard_map/dot_general | solution.py:1239
  35.2 0.0 copy-start.2
  35.2 0.0 copy-start.5
  35.3 0.0 copy-done.1
  35.3 0.0 copy-done.3
  35.3 0.0 copy-start.6
  35.3 0.0 copy-start.4
  35.3 0.0 copy-start.7
  35.3 0.9 multiply_reduce_fusion
  36.2 0.1 copy-done.2
  36.3 0.0 copy-done.5
  36.3 0.4 fusion
  36.7 0.0 copy-start
  36.7 0.0 copy-done.6
  36.7 1.0 fusion.2.normed_ref
  37.7 0.0 copy-done.4
  37.7 0.1 fusion.3
  37.9 0.0 copy-done.7
  37.9 0.6 maximum_bitcast_fusion.slots_ref
  38.5 0.0 copy-done
  38.5 137.2 %expert_layer.1 = bf16[128,2048]{1,0:T(8,128)(2,1)} custom-call(bf16[128,2048]{1,0:T(8,128)(2,1)} %fusion.2.normed_ref, f32[8,128]{1,0:T(8,128)} %maximum_bitcast_fusion.slots_ref, bf16[2,2048,256]{2,1,0:T(8,128)(2,1)} %gate_ref.1, bf16[2,2048,256]{2,1,0:T(8,128)(2,1)} %up_ref.1, bf16[2,256,2048]{2,1,0:T(8,128)(2,1)} %down_ref.1, ...), custom_call_target="tpu_custom_call" | custom-call | tf_op jit(solution)/shard_map/expert_layer/pallas_call | solution.py:1154
  175.7 1.9 %copy.28 = bf16[128,2048]{1,0:T(8,128)(2,1)} copy(bf16[128,2048]{1,0:T(8,128)(2,1)} %expert_layer.1) | data formatting | bytes 1048576
  (5 shorter events, 0.1 us)
Async XLA Ops:
  0.0 35.3 %copy-start.1 = (bf16[1024,2048]{1,0:T(8,128)(2,1)S(1)}, bf16[1024,2048]{1,0:T(8,128)(2,1)}, u32[]{:S(2)}) copy-start(bf16[1024,2048]{1,0:T(8,128)(2,1)} %param.35) | copy-start | bytes 12582916
  32.2 3.1 %copy-start.3 = (bf16[128,1024]{1,0:T(8,128)(2,1)S(1)}, bf16[128,1024]{1,0:T(8,128)(2,1)}, u32[]{:S(2)}) copy-start(bf16[128,1024]{1,0:T(8,128)(2,1)} %get-tuple-element.8) | copy-start | bytes 786436
  35.2 1.0 copy-start.2
  35.2 1.0 copy-start.5
  35.3 1.4 copy-start.6
  35.3 2.4 %copy-start.4 = (s32[128,4]{0,1:T(4,128)S(1)}, s32[128,4]{0,1:T(4,128)}, u32[]{:S(2)}) copy-start(s32[128,4]{0,1:T(4,128)} %param.46) | copy-start | bytes 6148
  35.3 2.6 %copy-start.7 = (f32[128,4]{0,1:T(4,128)S(1)}, f32[128,4]{0,1:T(4,128)}, u32[]{:S(2)}) copy-start(f32[128,4]{0,1:T(4,128)} %param.47) | copy-start | bytes 6148
  36.7 1.8 %copy-start = (bf16[128,2048]{1,0:T(8,128)(2,1)}, bf16[128,2048]{1,0:T(8,128)(2,1)S(1)}, u32[]{:S(2)}) copy-start(bf16[128,2048]{1,0:T(8,128)(2,1)S(1)} %get-tuple-element.10.mixed_ref) | copy-start | bytes 1572868

commit v5 on v4

--- a/solution.py
+++ b/solution.py
@@ -1069,6 +1069,10 @@
         each(distance, arrive)
         each(distance, select)
 
+        @pl.when(at_edge & (planes > 2) & (distance == planes - 1))
+        def _():
+            gather_up(first_out, False)
+
         @pl.when(distance > 1)
         def _():
             each(distance - 1, process)
@@ -1076,10 +1080,6 @@
         return carry
 
     lax.fori_loop(1, planes, step, 0)
-
-    @pl.when(at_edge & (planes > 2))
-    def _():
-        gather_up(first_out, False)
 
     each(planes - 1, process)
     hand_back(plane)

time: 178 us -> 177 us (level)
  no operation moved by 1% of the time
where the time goes in v5:
time: 177 us
  Pallas kernels  168 us (95%)
  matrix products  4.04 us (2%)
  other arithmetic  2.03 us (1%)
  local copies, waits for them, and re-layouts  2 us (1%)
    pallas_call x1, Pallas kernels, expert_rows(): pl.pallas_call(functools.partial(expert_kernel, dims, group, chunks), out...  136 us
    pallas_call x1, Pallas kernels, attended_rows(): pl.pallas_call(functools.partial(attend_kernel, (planes, rows, columns, t...  32.2 us

profile of v5, /device:TPU:0, one launch (start us, length us, event | category | flops | bytes accessed | tf_op | source)
XLA Modules:
  0.0 176.6 jit_solution(4695414429588824705)
XLA Ops:
  0.0 0.0 copy-start.1
  0.0 32.2 %gather_attend.1 = (bf16[128,1024]{1,0:T(8,128)(2,1)}, bf16[128,1024]{1,0:T(8,128)(2,1)}) custom-call(bf16[256,512]{1,0:T(8,128)(2,1)} %qn_ref.1, bf16[256,128]{1,0:T(8,128)(2,1)} %kn_ref.1, bf16[256,128]{1,0:T(8,128)(2,1)} %vn_ref.1, bf16[256,512]{1,0:T(8,128)(2,1)} %qw_ref.1, bf16[256,256]{1,0:T(8,128)(2,1)} %kw_ref.1, bf16[256,256]{1,0:T(8,128)(2,1)} %vw_ref.1, ...), custom_call_target="tpu_custom_call" | custom-call | tf_op jit(solution)/shard_map/gather_attend/pallas_call | solution.py:608
  32.2 0.0 copy-start.3
  32.2 3.0 %fusion.5 = f32[128,2048]{1,0:T(8,128)S(1)} fusion(bf16[128,1024]{1,0:T(8,128)(2,1)} %get-tuple-element.7, bf16[1024,2048]{1,0:T(8,128)(2,1)} %param.34), kind=kOutput, calls=%fused_computation.18 | convolution fusion | flops 536870912 | bytes 5505024 | tf_op jit(solution)/shard_map/dot_general | solution.py:1239
  35.2 0.0 copy-start.2
  35.2 0.0 copy-start.5
  35.3 0.0 copy-done.1
  35.3 0.0 copy-done.3
  35.3 0.0 copy-start.6
  35.3 0.0 copy-start.4
  35.3 0.0 copy-start.7
  35.3 0.9 multiply_reduce_fusion
  36.2 0.1 copy-done.2
  36.3 0.0 copy-done.5
  36.3 0.4 fusion
  36.7 0.0 copy-start
  36.7 0.0 copy-done.6
  36.7 1.0 fusion.2.normed_ref
  37.7 0.0 copy-done.4
  37.7 0.1 fusion.3
  37.9 0.0 copy-done.7
  37.9 0.6 maximum_bitcast_fusion.slots_ref
  38.5 0.0 copy-done
  38.5 136.3 %expert_layer.1 = bf16[128,2048]{1,0:T(8,128)(2,1)} custom-call(bf16[128,2048]{1,0:T(8,128)(2,1)} %fusion.2.normed_ref, f32[8,128]{1,0:T(8,128)} %maximum_bitcast_fusion.slots_ref, bf16[2,2048,256]{2,1,0:T(8,128)(2,1)} %gate_ref.1, bf16[2,2048,256]{2,1,0:T(8,128)(2,1)} %up_ref.1, bf16[2,256,2048]{2,1,0:T(8,128)(2,1)} %down_ref.1, ...), custom_call_target="tpu_custom_call" | custom-call | tf_op jit(solution)/shard_map/expert_layer/pallas_call | solution.py:1154
  174.8 1.9 %copy.28 = bf16[128,2048]{1,0:T(8,128)(2,1)} copy(bf16[128,2048]{1,0:T(8,128)(2,1)} %expert_layer.1) | data formatting | bytes 1048576
  (5 shorter events, 0.1 us)
Async XLA Ops:
  0.0 35.3 %copy-start.1 = (bf16[1024,2048]{1,0:T(8,128)(2,1)S(1)}, bf16[1024,2048]{1,0:T(8,128)(2,1)}, u32[]{:S(2)}) copy-start(bf16[1024,2048]{1,0:T(8,128)(2,1)} %param.35) | copy-start | bytes 12582916
  32.2 3.1 %copy-start.3 = (bf16[128,1024]{1,0:T(8,128)(2,1)S(1)}, bf16[128,1024]{1,0:T(8,128)(2,1)}, u32[]{:S(2)}) copy-start(bf16[128,1024]{1,0:T(8,128)(2,1)} %get-tuple-element.8) | copy-start | bytes 786436
  35.2 1.0 copy-start.2
  35.2 1.0 copy-start.5
  35.3 1.4 copy-start.6
  35.3 2.4 %copy-start.4 = (s32[128,4]{0,1:T(4,128)S(1)}, s32[128,4]{0,1:T(4,128)}, u32[]{:S(2)}) copy-start(s32[128,4]{0,1:T(4,128)} %param.46) | copy-start | bytes 6148
  35.3 2.6 %copy-start.7 = (f32[128,4]{0,1:T(4,128)S(1)}, f32[128,4]{0,1:T(4,128)}, u32[]{:S(2)}) copy-start(f32[128,4]{0,1:T(4,128)} %param.47) | copy-start | bytes 6148
  36.7 1.8 %copy-start = (bf16[128,2048]{1,0:T(8,128)(2,1)}, bf16[128,2048]{1,0:T(8,128)(2,1)S(1)}, u32[]{:S(2)}) copy-start(bf16[128,2048]{1,0:T(8,128)(2,1)S(1)} %get-tuple-element.10.mixed_ref) | copy-start | bytes 1572868

commit v6 on v5

--- a/solution.py
+++ b/solution.py
@@ -1045,8 +1045,9 @@
     at_edge = (plane == 0) | (plane == planes - 1)
     first_out = jnp.where(plane == 0, 1, planes - 2)
 
-    finish(plane)
-    experts(plane)
+    if planes == 1:
+        finish(plane)
+        experts(plane)
 
     def process(source):
         finish(source)
@@ -1072,6 +1073,11 @@
         @pl.when(at_edge & (planes > 2) & (distance == planes - 1))
         def _():
             gather_up(first_out, False)
+
+        @pl.when(distance == 1)
+        def _():
+            finish(plane)
+            experts(plane)
 
         @pl.when(distance > 1)
         def _():

time: 177 us -> 176 us (level)
  no operation moved by 1% of the time
where the time goes in v6:
time: 176 us
  Pallas kernels  168 us (95%)
  matrix products  4.04 us (2%)
  other arithmetic  2.03 us (1%)
  local copies, waits for them, and re-layouts  2 us (1%)
    pallas_call x1, Pallas kernels, expert_rows(): pl.pallas_call(functools.partial(expert_kernel, dims, group, chunks), out...  135 us
    pallas_call x1, Pallas kernels, attended_rows(): pl.pallas_call(functools.partial(attend_kernel, (planes, rows, columns, t...  32.2 us

profile of v6, /device:TPU:0, one launch (start us, length us, event | category | flops | bytes accessed | tf_op | source)
XLA Modules:
  0.0 175.8 jit_solution(16780627287047425747)
XLA Ops:
  0.0 0.0 copy-start.1
  0.0 32.2 %gather_attend.1 = (bf16[128,1024]{1,0:T(8,128)(2,1)}, bf16[128,1024]{1,0:T(8,128)(2,1)}) custom-call(bf16[256,512]{1,0:T(8,128)(2,1)} %qn_ref.1, bf16[256,128]{1,0:T(8,128)(2,1)} %kn_ref.1, bf16[256,128]{1,0:T(8,128)(2,1)} %vn_ref.1, bf16[256,512]{1,0:T(8,128)(2,1)} %qw_ref.1, bf16[256,256]{1,0:T(8,128)(2,1)} %kw_ref.1, bf16[256,256]{1,0:T(8,128)(2,1)} %vw_ref.1, ...), custom_call_target="tpu_custom_call" | custom-call | tf_op jit(solution)/shard_map/gather_attend/pallas_call | solution.py:608
  32.2 0.0 copy-start.3
  32.2 3.0 %fusion.5 = f32[128,2048]{1,0:T(8,128)S(1)} fusion(bf16[128,1024]{1,0:T(8,128)(2,1)} %get-tuple-element.7, bf16[1024,2048]{1,0:T(8,128)(2,1)} %param.34), kind=kOutput, calls=%fused_computation.18 | convolution fusion | flops 536870912 | bytes 5505024 | tf_op jit(solution)/shard_map/dot_general | solution.py:1245
  35.2 0.0 copy-start.2
  35.2 0.0 copy-start.5
  35.3 0.0 copy-done.1
  35.3 0.0 copy-done.3
  35.3 0.0 copy-start.6
  35.3 0.0 copy-start.4
  35.3 0.0 copy-start.7
  35.3 0.9 multiply_reduce_fusion
  36.2 0.1 copy-done.2
  36.3 0.0 copy-done.5
  36.3 0.4 fusion
  36.7 0.0 copy-start
  36.7 0.0 copy-done.6
  36.7 1.0 fusion.2.normed_ref
  37.7 0.0 copy-done.4
  37.7 0.1 fusion.3
  37.9 0.0 copy-done.7
  37.9 0.6 maximum_bitcast_fusion.slots_ref
  38.5 0.0 copy-done
  38.5 135.5 %expert_layer.1 = bf16[128,2048]{1,0:T(8,128)(2,1)} custom-call(bf16[128,2048]{1,0:T(8,128)(2,1)} %fusion.2.normed_ref, f32[8,128]{1,0:T(8,128)} %maximum_bitcast_fusion.slots_ref, bf16[2,2048,256]{2,1,0:T(8,128)(2,1)} %gate_ref.1, bf16[2,2048,256]{2,1,0:T(8,128)(2,1)} %up_ref.1, bf16[2,256,2048]{2,1,0:T(8,128)(2,1)} %down_ref.1, ...), custom_call_target="tpu_custom_call" | custom-call | tf_op jit(solution)/shard_map/expert_layer/pallas_call | solution.py:1160
  174.0 1.9 %copy.28 = bf16[128,2048]{1,0:T(8,128)(2,1)} copy(bf16[128,2048]{1,0:T(8,128)(2,1)} %expert_layer.1) | data formatting | bytes 1048576
  (5 shorter events, 0.1 us)
Async XLA Ops:
  0.0 35.3 %copy-start.1 = (bf16[1024,2048]{1,0:T(8,128)(2,1)S(1)}, bf16[1024,2048]{1,0:T(8,128)(2,1)}, u32[]{:S(2)}) copy-start(bf16[1024,2048]{1,0:T(8,128)(2,1)} %param.35) | copy-start | bytes 12582916
  32.2 3.1 %copy-start.3 = (bf16[128,1024]{1,0:T(8,128)(2,1)S(1)}, bf16[128,1024]{1,0:T(8,128)(2,1)}, u32[]{:S(2)}) copy-start(bf16[128,1024]{1,0:T(8,128)(2,1)} %get-tuple-element.8) | copy-start | bytes 786436
  35.2 1.0 copy-start.2
  35.2 1.0 copy-start.5
  35.3 1.4 copy-start.6
  35.3 2.4 %copy-start.4 = (s32[128,4]{0,1:T(4,128)S(1)}, s32[128,4]{0,1:T(4,128)}, u32[]{:S(2)}) copy-start(s32[128,4]{0,1:T(4,128)} %param.46) | copy-start | bytes 6148
  35.3 2.6 %copy-start.7 = (f32[128,4]{0,1:T(4,128)S(1)}, f32[128,4]{0,1:T(4,128)}, u32[]{:S(2)}) copy-start(f32[128,4]{0,1:T(4,128)} %param.47) | copy-start | bytes 6148
  36.7 1.8 %copy-start = (bf16[128,2048]{1,0:T(8,128)(2,1)}, bf16[128,2048]{1,0:T(8,128)(2,1)S(1)}, u32[]{:S(2)}) copy-start(bf16[128,2048]{1,0:T(8,128)(2,1)S(1)} %get-tuple-element.10.mixed_ref) | copy-start | bytes 1572868
